TPU v7x, 128 devices: a whole 4x4x4 slice. The times are simulated.
128 devices in a mesh: ep: 32 (over z, y, core), tp: 4 (over x).
Axes of the slice: x: 4, y: 4, z: 4, core: 2. Of those that a mesh axis runs over, the one named last changes fastest.
Arguments:
- mixer_input_rows: bfloat16 [16384, 2048], P(('ep', 'tp')), may hold values from -6 to 6
- mixer_norm_scale: float32 [2048], replicated, may hold values from 0.1 to 1.9
- decay_bias_table: float32 [16384, 16], P('ep', 'tp'), may hold values from -14 to 1
- erase_bias_table: float32 [16], P('tp'), may hold values from -12 to 1
- receive_weight: bfloat16 [2048, 1024], P(None, 'tp'), may hold values from -0.125 to 0.125
- key_weight: bfloat16 [2048, 1024], P(None, 'tp'), may hold values from -0.125 to 0.125
- value_weight: bfloat16 [2048, 1024], P(None, 'tp'), may hold values from -0.125 to 0.125
- decay_weight: bfloat16 [2048, 1024], P(None, 'tp'), may hold values from -0.125 to 0.125
- erase_weight: bfloat16 [2048, 1024], P(None, 'tp'), may hold values from -0.125 to 0.125
- self_token_scale: float32 [16, 64], P('tp'), may hold values from -0.6 to 0.6
- head_norm_scale: float32 [1024], P('tp'), may hold values from 0.1 to 1.9
- output_weight: bfloat16 [1024, 2048], P('tp'), may hold values from -0.1875 to 0.1875
- expert_input_rows: bfloat16 [16384, 2048], P(('ep', 'tp')), may hold values from -6 to 6
- expert_norm_scale: float32 [2048], replicated, may hold values from 0.1 to 1.9
- routes: int32 [16384, 2], P(('ep', 'tp')), may hold values from 0 to 127, all different within a row; in each aligned block of 128 rows (0 to 127, 128 to 255, ...) at most 4 rows name the same one
- router_weights: float32 [16384, 2], P(('ep', 'tp')), may hold values from 0.1 to 1
- routed_gate_weight: bfloat16 [128, 2048, 1024], P(('ep', 'tp')), may hold values from -0.125 to 0.125
- routed_up_weight: bfloat16 [128, 2048, 1024], P(('ep', 'tp')), may hold values from -0.125 to 0.125
- routed_down_weight: bfloat16 [128, 1024, 2048], P(('ep', 'tp')), may hold values from -0.1875 to 0.1875
- common_gate_weight: bfloat16 [2048, 256], replicated, may hold values from -0.125 to 0.125
- common_up_weight: bfloat16 [2048, 256], replicated, may hold values from -0.125 to 0.125
- common_down_weight: bfloat16 [256, 2048], replicated, may hold values from -0.375 to 0.375
Outputs:
- mixer_output: bfloat16 [16384, 2048], P(('ep', 'tp'))
- mixed_b: bfloat16 [16384, 2048], P(('ep', 'tp'))
Inputs may be any that keep to these rules, and one draw needn't show every extreme that they name: `routes`: within the rows of one device no expert is named by more than 4 rows, a bound that some block reaches; each row names 2 different experts, and every expert is named somewhere.
All inputs are finite; a program needn't handle non-finite values.
Results may differ from a plain program's by a relative error of at most 0.015.
Values may be sent and summed in bfloat16 or wider, within the bound.
A program may use at most 128 MiB of HBM per device.

v0:
```python
import jax
import jax.numpy as jnp
from jax import lax
from jax.sharding import Mesh
from jax.sharding import PartitionSpec as P

EP = ("ep_0", "ep_1", "ep_2")
EP_TP = ("ep_0", "ep_1", "ep_2", "tp")


def copy_for_each(value, axis):
    copies = jnp.broadcast_to(value, (lax.axis_size(axis), *value.shape))
    return lax.all_to_all(copies, axis, split_axis=0, concat_axis=0, tiled=True)


def laid_out(blocks, dim):
    dims = list(blocks.shape[1:])
    dims[dim] *= blocks.shape[0]
    return jnp.moveaxis(blocks, 0, dim).reshape(dims)


def gathered_copies(value, axis, dim):
    blocks = copy_for_each(value, axis)
    return laid_out(blocks, dim)


def filled_with(value, identity):
    return jax.tree.map(
        lambda a, e: jnp.broadcast_to(jnp.asarray(e, a.dtype), a.shape), value, identity
    )


def entering_2(value, axes, combine, identity):
    before = start = filled_with(value, identity)
    so_far = value
    for axis in reversed(axes):
        peers, here = (lax.axis_size(axis), lax.axis_index(axis))
        pieces = jax.tree.map(
            lambda part, kind: lax.all_gather(part.astype(kind), axis),
            so_far,
            (jnp.bfloat16, jnp.bfloat16),
        )
        inside, so_far = (start, start)
        for k in range(peers):
            passed = k < here
            so_far = combine(
                so_far, jax.tree.map(lambda part, own: part[k].astype(own.dtype), pieces, value)
            )
            inside = jax.tree.map(lambda new, old: jnp.where(passed, new, old), so_far, inside)
        before = combine(inside, before)
    return before


def cut_along(value, dim, peers):
    before, after = (value.shape[:dim], value.shape[dim + 1 :])
    return jnp.moveaxis(value.reshape(*before, peers, -1, *after), dim, 0)


def summed_on_arrival(value, axis, dim):
    blocks = cut_along(value, dim, lax.axis_size(axis))
    arrived = lax.all_to_all(blocks, axis, split_axis=0, concat_axis=0, tiled=True)
    return arrived.astype(jnp.float32).sum(axis=0)


def one_exchange(value, axis, axes, splits, concats):
    sizes = [lax.axis_size(a) for a in axes]
    blocks = cut_along(value, splits[0], sizes[0])
    blocks = jnp.moveaxis(cut_along(blocks, splits[1] + 1, sizes[1]), 0, 1)
    inside = blocks.shape[2:]
    blocks = blocks.reshape(-1, *inside)
    blocks = lax.all_to_all(blocks, axis, split_axis=0, concat_axis=0, tiled=True)
    blocks = laid_out(blocks.reshape(*sizes, *inside), concats[0] + 1)
    return laid_out(blocks, concats[1])


def rms_rows(values, feature_gain):
    wide_values = values.astype(jnp.float32)
    inverse = lax.rsqrt(jnp.mean(wide_values * wide_values, axis=1, keepdims=True) + 1e-06)
    return (wide_values * inverse * feature_gain).astype(jnp.bfloat16)


def masked_pairs(left_rows, right_rows, keep_mask):
    products = jnp.einsum("htk,hsk->hts", left_rows, right_rows)
    return jnp.where(keep_mask[None], products, 0.0)


def block_pass(state_in, inputs):
    receive_vector, log_decay, key_projected, value_projected, unit_key, erase_rate = inputs
    block_len = receive_vector.shape[1]
    positions = jnp.arange(block_len)
    strict_mask = positions[:, None] > positions[None, :]
    causal_mask = positions[:, None] >= positions[None, :]
    cumulative = jnp.cumsum(log_decay, axis=1)
    growth = jnp.exp(-cumulative)
    erase_in = -unit_key * jnp.exp(cumulative - log_decay)
    erase_out = unit_key * erase_rate * growth
    key_out = key_projected * growth
    read_in = receive_vector * jnp.exp(cumulative)
    value_aug = jnp.concatenate([value_projected, jnp.zeros_like(value_projected)], axis=2)
    mix_erase = masked_pairs(erase_in, erase_out, strict_mask)
    mix_key = masked_pairs(erase_in, key_out, strict_mask)
    read_erase = masked_pairs(read_in, erase_out, causal_mask)
    read_key = masked_pairs(read_in, key_out, causal_mask)
    right_side = jnp.einsum("hvk,htk->htv", state_in, erase_in) + jnp.einsum(
        "hts,hsv->htv", mix_key, value_aug
    )
    system = jnp.eye(block_len, dtype=jnp.float32)[None] - mix_erase
    erased = jax.scipy.linalg.solve_triangular(system, right_side, lower=True, unit_diagonal=True)
    outputs = (
        jnp.einsum("hvk,htk->htv", state_in, read_in)
        + jnp.einsum("hts,hsv->htv", read_erase, erased)
        + jnp.einsum("hts,hsv->htv", read_key, value_aug)
    )
    decay_tail = jnp.exp(cumulative[:, -1:, :] - cumulative)
    state_out = (
        state_in * jnp.exp(cumulative[:, -1, :])[:, None, :]
        + jnp.einsum("htv,htk->hvk", erased, unit_key * erase_rate * decay_tail)
        + jnp.einsum("htv,htk->hvk", value_aug, key_projected * decay_tail)
    )
    return (state_out, outputs)


def local_states(receive_vector, log_decay, key_projected, value_projected, unit_key, erase_rate):
    row_count, head_count, head_channel_count = receive_vector.shape
    block_len = min(64, row_count)
    block_count = row_count // block_len

    def blocked(field_rows):
        return field_rows.reshape(block_count, block_len, head_count, head_channel_count).transpose(
            0, 2, 1, 3
        )

    identity_part = jnp.broadcast_to(
        jnp.eye(head_channel_count, dtype=jnp.float32),
        (head_count, head_channel_count, head_channel_count),
    )
    start_state = jnp.concatenate(
        [
            jnp.zeros((head_count, head_channel_count, head_channel_count), jnp.float32),
            identity_part,
        ],
        axis=1,
    )
    members = (receive_vector, log_decay, key_projected, value_projected, unit_key, erase_rate)
    final_state, outputs = lax.scan(
        block_pass, start_state, tuple((blocked(member) for member in members))
    )
    outputs = outputs.transpose(0, 2, 1, 3).reshape(row_count, head_count, 2 * head_channel_count)
    return (final_state, outputs)


def per_device(
    mixer_input_rows,
    mixer_norm_scale,
    decay_bias_table,
    erase_bias_table,
    receive_weight,
    key_weight,
    value_weight,
    decay_weight,
    erase_weight,
    self_token_scale,
    head_norm_scale,
    output_weight,
    expert_input_rows,
    expert_norm_scale,
    routes,
    router_weights,
    routed_gate_weight,
    routed_up_weight,
    routed_down_weight,
    common_gate_weight,
    common_up_weight,
    common_down_weight,
):
    normed_a = rms_rows(mixer_input_rows, mixer_norm_scale)
    local_width = key_weight.shape[1]
    row_piece = gathered_copies(normed_a, "tp", 0)
    projected = jnp.concatenate(
        [
            jnp.dot(row_piece, weight_part, preferred_element_type=jnp.float32)
            for weight_part in (
                receive_weight,
                key_weight,
                value_weight,
                decay_weight,
                erase_weight,
            )
        ],
        axis=1,
    )
    row_count = projected.shape[0]
    head_channel_count = self_token_scale.shape[1]
    head_count = local_width // head_channel_count

    def head_slice(index_part):
        columns = projected[:, index_part * local_width : (index_part + 1) * local_width]
        return columns.reshape(row_count, head_count, head_channel_count)

    receive_vector = head_slice(0)
    key_projected = head_slice(1)
    value_projected = head_slice(2)
    log_decay = -jnp.exp(-jax.nn.softplus(-(head_slice(3) + decay_bias_table[:, :, None])) - 0.5)
    erase_rate = jax.nn.sigmoid(head_slice(4) + erase_bias_table[None, :, None])
    unit_key = key_projected * lax.rsqrt(
        jnp.sum(key_projected * key_projected, axis=2, keepdims=True) + 1e-06
    )
    final_state, outputs = local_states(
        receive_vector, log_decay, key_projected, value_projected, unit_key, erase_rate
    )
    state_local = final_state[:, :head_channel_count]
    transit = final_state[:, head_channel_count:]

    def compose(earlier_part, later_part):
        joined = jnp.einsum("hij,hjk->hik", earlier_part[0], later_part[0])
        summed = jnp.einsum("hvj,hjk->hvk", earlier_part[1], later_part[0]) + later_part[1]
        return (joined, summed)

    identity = (
        jnp.broadcast_to(jnp.eye(head_channel_count, dtype=jnp.float32), transit.shape),
        jnp.zeros_like(state_local),
    )
    entering = entering_2((transit, state_local), EP, compose, identity)[1]
    readout = outputs[:, :, :head_channel_count] + jnp.einsum(
        "hvk,thk->thv", entering, outputs[:, :, head_channel_count:]
    )
    mean_removed = readout - jnp.mean(readout, axis=2, keepdims=True)
    squared_mean = jnp.mean(mean_removed * mean_removed, axis=2, keepdims=True)
    head_norm_scales = head_norm_scale.reshape(head_count, head_channel_count)
    self_token_term = (
        jnp.sum(receive_vector * key_projected * self_token_scale[None], axis=2, keepdims=True)
        * value_projected
    )
    mixer_head_count = (
        mean_removed * lax.rsqrt(squared_mean + 0.00064) * head_norm_scales + self_token_term
    )
    mixer_head_count = mixer_head_count.reshape(row_count, local_width).astype(jnp.bfloat16)
    mixer_output = summed_on_arrival(
        jnp.dot(mixer_head_count, output_weight, preferred_element_type=jnp.float32).astype(
            jnp.bfloat16
        ),
        "tp",
        0,
    ).astype(jnp.bfloat16)
    normed_b = rms_rows(expert_input_rows, expert_norm_scale)
    route_weight = 2.5 * router_weights / jnp.sum(router_weights, axis=1, keepdims=True)
    token_count, top_count = routes.shape
    expert_count = lax.axis_size(EP) * lax.axis_size("tp")
    capacity = 2 * token_count * top_count // expert_count
    chosen = routes.reshape(-1)
    onehot = (chosen[:, None] == jnp.arange(expert_count, dtype=jnp.int32)[None, :]).astype(
        jnp.int32
    )
    slot_rank = jnp.sum(jnp.cumsum(onehot, axis=0) * onehot, axis=1) - 1
    slot_index = chosen * capacity + slot_rank
    owners = jnp.arange(token_count * top_count, dtype=jnp.int32) // top_count
    source_row = jnp.zeros((expert_count * capacity,), jnp.int32).at[slot_index].set(owners)
    filled = jnp.zeros((expert_count * capacity,), jnp.bfloat16).at[slot_index].set(1.0)
    outgoing = (normed_b[source_row] * filled[:, None]).reshape(expert_count, capacity, -1)
    gate_part = routed_gate_weight[0]
    up_part = routed_up_weight[0]
    down_part = routed_down_weight[0]
    grouped = outgoing.reshape(lax.axis_size(EP), lax.axis_size("tp"), capacity, -1)
    arrived = one_exchange(grouped, EP_TP, (EP, "tp"), (0, 1), (0, 1))
    flat_rows = arrived.reshape(-1, arrived.shape[-1])
    expert_hidden = (
        jax.nn.silu(jnp.dot(flat_rows, gate_part, preferred_element_type=jnp.float32))
        * jnp.dot(flat_rows, up_part, preferred_element_type=jnp.float32)
    ).astype(jnp.bfloat16)
    result = jnp.dot(expert_hidden, down_part, preferred_element_type=jnp.float32).astype(
        jnp.bfloat16
    )
    returned = one_exchange(result.reshape(arrived.shape), EP_TP, (EP, "tp"), (0, 1), (0, 1))
    back_rows = returned.reshape(expert_count * capacity, -1)
    picked = back_rows[slot_index].reshape(token_count, top_count, -1)
    routed = jnp.sum(picked * route_weight[:, :, None], axis=1)
    shared_hidden = (
        jax.nn.silu(jnp.dot(normed_b, common_gate_weight, preferred_element_type=jnp.float32))
        * jnp.dot(normed_b, common_up_weight, preferred_element_type=jnp.float32)
    ).astype(jnp.bfloat16)
    shared_term = jnp.dot(shared_hidden, common_down_weight, preferred_element_type=jnp.float32)
    mixed_b = (routed + shared_term).astype(jnp.bfloat16)
    return (mixer_output, mixed_b)


def solution(mesh):
    split = Mesh(mesh.devices.reshape(4, 4, 2, mesh.shape["tp"]), ("ep_0", "ep_1", "ep_2", "tp"))
    in_specs = (
        P(EP_TP, None),
        P(),
        P(EP, "tp"),
        P("tp"),
        P(None, "tp"),
        P(None, "tp"),
        P(None, "tp"),
        P(None, "tp"),
        P(None, "tp"),
        P("tp", None),
        P("tp"),
        P("tp", None),
        P(EP_TP, None),
        P(),
        P(EP_TP, None),
        P(EP_TP, None),
        P(EP_TP, None, None),
        P(EP_TP, None, None),
        P(EP_TP, None, None),
        P(),
        P(),
        P(),
    )
    out_specs = (P(EP_TP, None), P(EP_TP, None))
    return jax.shard_map(
        per_device, mesh=split, in_specs=in_specs, out_specs=out_specs, check_vma=False
    )
```

profile of v0, /device:TPU:1, one launch (start us, length us, event | category | flops | bytes accessed | tf_op | source)
XLA Modules:
  0.0 482.8 jit_solution(17119804915335986662)
XLA Ops:
  4.8 5.0 %all-to-all-start = ((bf16[4,128,2048]{2,1,0:T(8,128)(2,1)}), bf16[4,128,2048]{2,1,0:T(8,128)(2,1)}, u32[]{:S(2)}, u32[]{:S(2)}) async-start(bf16[4,128,2048]{2,1,0:T(8,128)(2,1)} %broadcast_in_dim.95), calls=%async_computation | async-start | bytes 4194304 | tf_op jit(solution)/shard_map/all_to_all | solution.py:13
  16.8 3.3 gather_fusion
  20.2 4.1 gather.9
  26.7 3.9 bitcast_multiply_fusion.20
  30.6 5.1 %all-to-all-done = bf16[4,128,2048]{2,1,0:T(8,128)(2,1)} async-done(((bf16[4,128,2048]{2,1,0:T(8,128)(2,1)}), bf16[4,128,2048]{2,1,0:T(8,128)(2,1)}, u32[]{:S(2)}, u32[]{:S(2)}) %all-to-all-start) | async-done | bytes 2097184 | tf_op jit(solution)/shard_map/all_to_all | solution.py:13
  35.7 10.5 %all-to-all-start.2 = ((bf16[128,1,1,4,2048]{4,3,2,1,0:T(4,128)(2,1)}), bf16[128,1,1,4,2048]{4,3,2,1,0:T(4,128)(2,1)}, u32[]{:S(2)}, u32[]{:S(2)}) async-start(bf16[128,1,1,4,2048]{4,3,2,1,0:T(4,128)(2,1)} %bitcast_multiply_fusion.20), calls=%async_computation.2 | async-start | bytes 4194304 | tf_op jit(solution)/shard_map/all_to_all | solution.py:71
  53.1 3.5 fusion.177
  56.6 3.5 fusion.72
  64.3 3.5 fusion.48
  82.0 245.6 %while.12 = (s32[]{:T(128)}, f32[4,128,64]{1,2,0:T(8,128)S(1)}, f32[8,4,64,128]{3,2,0,1:T(8,128)}, f32[8,4,64,64]{3,2,1,0:T(8,128)}, f32[8,4,64,64]{3,2,1,0:T(8,...) while((s32[]{:T(128)}, f32[4,128,64]{1,2,0:T(8,128)S(1)}, ...), condition=%wide.region_4.5_spmd, body=%wide.region_2.4_spmd.sunk | while | flops 64614464 | bytes 5526681 | solution.py:145
  88.4 20.4 %custom-call.10 = f32[4,1,64,64]{2,3,1,0:T(8,128)S(1)} custom-call(f32[4,1,64,64]{3,2,1,0:T(8,128)} %fusion.255), custom_call_target="InvertDiagBlocksLowerTriangular" | custom-call | tf_op jit(solution)/shard_map/while/body/eval_jaxpr/jit(_solve_triangular)/vmap()/triangular_solve | solution.py:108
  119.1 20.4 %custom-call.10 = f32[4,1,64,64]{2,3,1,0:T(8,128)S(1)} custom-call(f32[4,1,64,64]{3,2,1,0:T(8,128)} %fusion.255), custom_call_target="InvertDiagBlocksLowerTriangular" | custom-call | tf_op jit(solution)/shard_map/while/body/eval_jaxpr/jit(_solve_triangular)/vmap()/triangular_solve | solution.py:108
  149.8 20.4 %custom-call.10 = f32[4,1,64,64]{2,3,1,0:T(8,128)S(1)} custom-call(f32[4,1,64,64]{3,2,1,0:T(8,128)} %fusion.255), custom_call_target="InvertDiagBlocksLowerTriangular" | custom-call | tf_op jit(solution)/shard_map/while/body/eval_jaxpr/jit(_solve_triangular)/vmap()/triangular_solve | solution.py:108
  180.5 20.4 %custom-call.10 = f32[4,1,64,64]{2,3,1,0:T(8,128)S(1)} custom-call(f32[4,1,64,64]{3,2,1,0:T(8,128)} %fusion.255), custom_call_target="InvertDiagBlocksLowerTriangular" | custom-call | tf_op jit(solution)/shard_map/while/body/eval_jaxpr/jit(_solve_triangular)/vmap()/triangular_solve | solution.py:108
  211.1 20.4 %custom-call.10 = f32[4,1,64,64]{2,3,1,0:T(8,128)S(1)} custom-call(f32[4,1,64,64]{3,2,1,0:T(8,128)} %fusion.255), custom_call_target="InvertDiagBlocksLowerTriangular" | custom-call | tf_op jit(solution)/shard_map/while/body/eval_jaxpr/jit(_solve_triangular)/vmap()/triangular_solve | solution.py:108
  241.8 20.4 %custom-call.10 = f32[4,1,64,64]{2,3,1,0:T(8,128)S(1)} custom-call(f32[4,1,64,64]{3,2,1,0:T(8,128)} %fusion.255), custom_call_target="InvertDiagBlocksLowerTriangular" | custom-call | tf_op jit(solution)/shard_map/while/body/eval_jaxpr/jit(_solve_triangular)/vmap()/triangular_solve | solution.py:108
  272.5 20.4 %custom-call.10 = f32[4,1,64,64]{2,3,1,0:T(8,128)S(1)} custom-call(f32[4,1,64,64]{3,2,1,0:T(8,128)} %fusion.255), custom_call_target="InvertDiagBlocksLowerTriangular" | custom-call | tf_op jit(solution)/shard_map/while/body/eval_jaxpr/jit(_solve_triangular)/vmap()/triangular_solve | solution.py:108
  303.2 20.4 %custom-call.10 = f32[4,1,64,64]{2,3,1,0:T(8,128)S(1)} custom-call(f32[4,1,64,64]{3,2,1,0:T(8,128)} %fusion.255), custom_call_target="InvertDiagBlocksLowerTriangular" | custom-call | tf_op jit(solution)/shard_map/while/body/eval_jaxpr/jit(_solve_triangular)/vmap()/triangular_solve | solution.py:108
  335.5 9.4 %all-gather.4 = bf16[16,64,64]{2,1,0:T(8,128)(2,1)S(1)} all-gather(bf16[4,64,64]{2,1,0:T(8,128)(2,1)S(1)} %convolution_add_fusion.14), channel_id=6, replica_groups=mesh['ep_0'=4,'ep_1'=4,'ep_2'=2,'tp'=4] {'ep_1'}, dimensions={0}, use_global_device_ids=true | all-gather | bytes 163840 | tf_op jit(solution)/shard_map/all_gather | solution.py:39
  344.9 9.4 %all-gather.1 = bf16[16,64,64]{2,1,0:T(8,128)(2,1)S(1)} all-gather(bf16[4,64,64]{2,1,0:T(8,128)(2,1)S(1)} %fusion.158), channel_id=3, replica_groups=mesh['ep_0'=4,'ep_1'=4,'ep_2'=2,'tp'=4] {'ep_1'}, dimensions={0}, use_global_device_ids=true | all-gather | bytes 163840 | tf_op jit(solution)/shard_map/all_gather | solution.py:39
  355.0 10.4 %all-gather.5 = bf16[16,64,64]{2,1,0:T(8,128)(2,1)S(1)} all-gather(bf16[4,64,64]{2,1,0:T(8,128)(2,1)S(1)} %convolution_add_fusion.11), channel_id=7, replica_groups=mesh['ep_0'=4,'ep_1'=4,'ep_2'=2,'tp'=4] {'ep_0'}, dimensions={0}, use_global_device_ids=true | all-gather | bytes 163840 | tf_op jit(solution)/shard_map/all_gather | solution.py:39
  365.8 9.9 %all-gather.2 = bf16[16,64,64]{2,1,0:T(8,128)(2,1)S(1)} all-gather(bf16[4,64,64]{2,1,0:T(8,128)(2,1)S(1)} %fusion.147), channel_id=4, replica_groups=mesh['ep_0'=4,'ep_1'=4,'ep_2'=2,'tp'=4] {'ep_0'}, dimensions={0}, use_global_device_ids=true | all-gather | bytes 163840 | tf_op jit(solution)/shard_map/all_gather | solution.py:39
  384.1 4.4 all-to-all-start.1
  388.5 4.0 reshape_reshape.18
  392.5 6.5 %fusion.37 = f32[512,1024]{1,0:T(8,128)} fusion(bf16[512,2048]{1,0:T(8,128)(2,1)} %reshape_reshape.18, bf16[1,2048,1024]{2,1,0:T(8,128)(2,1)} %param.40), kind=kOutput, calls=%fused_computation.66 | convolution fusion | flops 2147483648 | bytes 8388608 | tf_op jit(solution)/shard_map/dot_general | solution.py:267
  399.0 10.6 %fusion.39 = bf16[512,2048]{1,0:T(8,128)(2,1)} fusion(bf16[1,1024,2048]{2,1,0:T(8,128)(2,1)} %param.42, f32[512,1024]{1,0:T(8,128)} %fusion.37, bf16[512,2048]{1,0:T(8,128)(2,1)} %reshape_reshape.18, bf16[1,2048,1024]{2,1,0:T(8,128)(2,1)} %param.41), kind=kOutput, calls=%fused_computation.68 | convolution fusion | flops 4299161600 | bytes 14680064 | tf_op jit(solution)/shard_map/dot_general | solution.py:270
  409.6 4.1 reshape_transpose_transpose_reshape_reshape_reshape.3
  413.7 20.2 %all-to-all-start.3 = ((bf16[128,1,1,4,2048]{4,3,2,1,0:T(4,128)(2,1)}), bf16[128,1,1,4,2048]{4,3,2,1,0:T(4,128)(2,1)}, u32[]{:S(2)}, u32[]{:S(2)}) async-start(bf16[128,1,1,4,2048]{4,3,2,1,0:T(4,128)(2,1)} %bitcast.231), calls=%async_computation.3 | async-start | bytes 4194304 | tf_op jit(solution)/shard_map/all_to_all | solution.py:71
  437.3 27.0 %all-to-all-done.3 = bf16[128,1,1,4,2048]{4,3,2,1,0:T(4,128)(2,1)} async-done(((bf16[128,1,1,4,2048]{4,3,2,1,0:T(4,128)(2,1)}), bf16[128,1,1,4,2048]{4,3,2,1,0:T(4,128)(2,1)}, u32[]{:S(2)}, u32[]{:S(2)}) %all-to-all-start.3) | async-done | bytes 2097184 | tf_op jit(solution)/shard_map/all_to_all | solution.py:71
  464.3 3.9 reshape_reshape.19
  468.3 4.2 gather_fusion.1
  474.9 4.8 multiply_reduce_fusion
  (301 shorter events, 146.8 us)
Async XLA Ops:
  0.6 381.3 %copy-start = (bf16[256,2048]{1,0:T(8,128)(2,1)S(1)}, bf16[256,2048]{1,0:T(8,128)(2,1)}, u32[]{:S(2)}) copy-start(bf16[256,2048]{1,0:T(8,128)(2,1)} %param.35) | copy-start | bytes 3145732
  4.8 5.0 %copy-start.19 = (s32[128,2]{0,1:T(2,128)S(1)}, s32[128,2]{0,1:T(2,128)}, u32[]{:S(2)}) copy-start(s32[128,2]{0,1:T(2,128)} %param.38) | copy-start | bytes 3076
  4.8 7.8 %copy-start.8 = (bf16[2048,256]{1,0:T(8,128)(2,1)S(1)}, bf16[2048,256]{1,0:T(8,128)(2,1)}, u32[]{:S(2)}) copy-start(bf16[2048,256]{1,0:T(8,128)(2,1)} %param.31) | copy-start | bytes 3145732
  4.8 30.9 %all-to-all-start = ((bf16[4,128,2048]{2,1,0:T(8,128)(2,1)}), bf16[4,128,2048]{2,1,0:T(8,128)(2,1)}, u32[]{:S(2)}, u32[]{:S(2)}) async-start(bf16[4,128,2048]{2,1,0:T(8,128)(2,1)} %broadcast_in_dim.95), calls=%async_computation | async-start | bytes 4194304 | tf_op jit(solution)/shard_map/all_to_all | solution.py:13
  12.5 3.8 copy-start.6
  12.6 3.7 copy-start.22
  12.6 3.8 copy-start.5
  12.6 4.0 copy-start.18
  30.6 15.6 %copy-start.23 = (bf16[2048,256]{1,0:T(8,128)(2,1)S(1)}, bf16[2048,256]{1,0:T(8,128)(2,1)}, u32[]{:S(2)}) copy-start(bf16[2048,256]{1,0:T(8,128)(2,1)} %param.30) | copy-start | bytes 3145732
  35.7 348.4 %all-to-all-start.2 = ((bf16[128,1,1,4,2048]{4,3,2,1,0:T(4,128)(2,1)}), bf16[128,1,1,4,2048]{4,3,2,1,0:T(4,128)(2,1)}, u32[]{:S(2)}, u32[]{:S(2)}) async-start(bf16[128,1,1,4,2048]{4,3,2,1,0:T(4,128)(2,1)} %bitcast_multiply_fusion.20), calls=%async_computation.2 | async-start | bytes 4194304 | tf_op jit(solution)/shard_map/all_to_all | solution.py:71
  46.2 3.3 copy-start.24
  53.0 3.5 copy-start.9
  53.0 3.5 copy-start.25
  61.3 3.0 copy-start.26
  327.6 5.4 %copy-start.7 = (f32[64,64]{1,0:T(8,128)S(1)}, f32[64,64]{1,0:T(8,128)}, u32[]{:S(2)}) copy-start(f32[64,64]{1,0:T(8,128)} %copy-done.6) | copy-start | bytes 49156
  354.4 11.3 %copy-start.14 = (bf16[4,64,64]{2,1,0:T(8,128)(2,1)}, bf16[4,64,64]{2,1,0:T(8,128)(2,1)S(1)}, u32[]{:S(2)}) copy-start(bf16[4,64,64]{2,1,0:T(8,128)(2,1)S(1)} %fusion.122) | copy-start | bytes 98308
  355.0 25.1 %copy-start.2 = (f32[8,4,64,128]{3,2,0,1:T(8,128)S(1)}, f32[8,4,64,128]{3,2,0,1:T(8,128)}, u32[]{:S(2)}) copy-start(f32[8,4,64,128]{3,2,0,1:T(8,128)} %get-tuple-element.50) | copy-start | bytes 3145732
  365.6 11.6 %copy-start.12 = (bf16[4,64,64]{2,1,0:T(8,128)(2,1)}, bf16[4,64,64]{2,1,0:T(8,128)(2,1)S(1)}, u32[]{:S(2)}) copy-start(bf16[4,64,64]{2,1,0:T(8,128)(2,1)S(1)} %fusion.150) | copy-start | bytes 98308
  365.8 11.4 %copy-start.13 = (bf16[4,64,64]{2,1,0:T(8,128)(2,1)}, bf16[4,64,64]{2,1,0:T(8,128)(2,1)S(1)}, u32[]{:S(2)}) copy-start(bf16[4,64,64]{2,1,0:T(8,128)(2,1)S(1)} %fusion.147) | copy-start | bytes 98308
  375.7 0.7 copy-start.11
  375.9 1.4 copy-start.17
  376.1 1.2 copy-start.16
  376.2 1.1 copy-start.15
  377.3 4.5 copy-start.3
  377.3 4.5 copy-start.21
  380.1 1.7 copy-start.4
  384.1 29.7 %all-to-all-start.1 = ((bf16[4,128,2048]{2,1,0:T(8,128)(2,1)}), bf16[4,128,2048]{2,1,0:T(8,128)(2,1)}, u32[]{:S(2)}, u32[]{:S(2)}) async-start(bf16[4,128,2048]{2,1,0:T(8,128)(2,1)} %bitcast.229), calls=%async_computation.1 | async-start | bytes 4194304 | tf_op jit(solution)/shard_map/all_to_all | solution.py:61
  413.7 20.2 %copy-start.20 = (f32[128,2]{0,1:T(2,128)S(1)}, f32[128,2]{0,1:T(2,128)}, u32[]{:S(2)}) copy-start(f32[128,2]{0,1:T(2,128)} %param.39) | copy-start | bytes 3076
  413.7 20.4 %copy-start.10 = (bf16[2048,256]{1,0:T(8,128)(2,1)S(1)}, bf16[2048,256]{1,0:T(8,128)(2,1)}, u32[]{:S(2)}) copy-start(bf16[2048,256]{1,0:T(8,128)(2,1)} %param.43) | copy-start | bytes 3145732
  413.7 50.6 %all-to-all-start.3 = ((bf16[128,1,1,4,2048]{4,3,2,1,0:T(4,128)(2,1)}), bf16[128,1,1,4,2048]{4,3,2,1,0:T(4,128)(2,1)}, u32[]{:S(2)}, u32[]{:S(2)}) async-start(bf16[128,1,1,4,2048]{4,3,2,1,0:T(4,128)(2,1)} %bitcast.231), calls=%async_computation.3 | async-start | bytes 4194304 | tf_op jit(solution)/shard_map/all_to_all | solution.py:71
  474.9 7.9 %copy-start.1 = (bf16[256,2048]{1,0:T(8,128)(2,1)S(1)}, bf16[256,2048]{1,0:T(8,128)(2,1)}, u32[]{:S(2)}) copy-start(bf16[256,2048]{1,0:T(8,128)(2,1)} %param.35) | copy-start | bytes 3145732
where the time goes:
time: 486 us; the launch traced here: 483 us
  other arithmetic  198 us (41%)
  matrix products  96 us (20%)
  local copies, waits for them, and re-layouts  71.5 us (15%)
  blocking collectives  43.8 us (9%)
  starting transfers between devices  40.1 us (8%)
  waiting for transfers between devices  32.1 us (7%)
    another operation x16, other arithmetic, block_pass(): jax.scipy.linalg.solve_triangular(system, right_side, lower=True, unit_di...  163 us
    all_gather x6, blocking collectives, entering_2(): lax.all_gather(part.astype(kind), axis)  43.8 us
    all_to_all x2, starting transfers between devices, one_exchange(): lax.all_to_all(blocks, axis, split_axis=0, concat_axis=0, tiled=True)  30.7 us
    all_to_all x2, waiting for transfers between devices, one_exchange(): lax.all_to_all(blocks, axis, split_axis=0, concat_axis=0, tiled=True)  27 us
    dot_general x5, matrix products, per_device(): jnp.dot(row_piece, weight_part, preferred_element_type=jnp.float32)  16.1 us
    dot_general x8, matrix products, block_pass(): jnp.einsum('hts,hsv->htv', read_key, value_aug)  15 us
    squeeze x16, local copies, waits for them, and re-layouts, local_states(): lax.scan(block_pass, start_state, tuple((blocked(member) for member in me...  14.1 us
    another operation x6, local copies, waits for them, and re-layouts, blocked(): field_rows.reshape(block_count, block_len, head_count, head_channel_count)  10.8 us
  transfers between devices with their start and end apart: 4, of which 2 were waited for; matrix products, arithmetic and copies ran while one was open for 71% of the time, Pallas kernels for 0%

commit v1 on v0

v1 whole, which is shorter than its diff:
```python
import functools

import jax
import jax.numpy as jnp
from jax import lax
from jax.experimental import pallas as pl
from jax.experimental.pallas import tpu as pltpu
from jax.sharding import Mesh
from jax.sharding import PartitionSpec as P

EP = ("ep_0", "ep_1", "ep_2")
EP_TP = ("ep_0", "ep_1", "ep_2", "tp")
MESH = pl.DeviceIdType.MESH
BF = jnp.bfloat16
F32 = jnp.float32
VMEM = pltpu.VMEM
CHUNK = 64
PAIR = 128


def mm(a, b):
    return lax.dot_general(a, b, (((1,), (0,)), ((), ())), preferred_element_type=F32)


def mm_t(a, b):
    return lax.dot_general(a, b, (((1,), (1,)), ((), ())), preferred_element_type=F32)


def mm_tn(a, b):
    return lax.dot_general(a, b, (((0,), (0,)), ((), ())), preferred_element_type=F32)


def split2(x):
    hi = x.astype(BF)
    lo = (x - hi.astype(F32)).astype(BF)
    return hi, lo


def iota(shape, dim):
    return lax.broadcasted_iota(jnp.int32, shape, dim)


def pair_mask():
    return (iota((PAIR, PAIR), 0) // 64) == (iota((PAIR, PAIR), 1) // 64)


def block_diag(x, mask):
    return jnp.concatenate([x, x], axis=0) * mask


def head_sums(x, mask):
    hi, lo = split2(x)
    return mm(hi, mask) + mm(lo, mask)


def mixer_kernel(
    rows_ref, wr_ref, wk_ref, wv_ref, wd_ref, we_ref, db_ref, eb_ref, st_ref,
    out_ref, rt_ref, self_ref, tl_ref,
    pr_ref, r_s, e_s, l_s, d_s,
):
    n_rows = rows_ref.shape[0]
    n_chunks = n_rows // CHUNK
    group = 4
    mask_b = pair_mask()
    mask = mask_b.astype(F32).astype(BF)
    for j, w in enumerate((wr_ref, wk_ref, wv_ref, wd_ref, we_ref)):
        pr_ref[:, j * 256 : (j + 1) * 256] = mm(rows_ref[...], w[...])

    t_i = iota((CHUNK, PAIR), 0)
    s_i = iota((CHUNK, PAIR), 1) % 64
    strict = t_i > s_i
    causal = t_i >= s_i
    eye = (t_i == s_i).astype(F32)
    lane_lo = iota((CHUNK, PAIR), 1) < 64
    tril = (iota((CHUNK, CHUNK), 0) >= iota((CHUNK, CHUNK), 1)).astype(F32).astype(BF)

    def do_group(g, carry):
        units = []
        for cc in range(group):
            for p in range(2):
                r0 = pl.multiple_of((g * group + cc) * CHUNK, CHUNK)
                rows = pl.ds(r0, CHUNK)
                lanes = slice(p * PAIR, (p + 1) * PAIR)
                col = lambda j: pr_ref[rows, j * 256 + p * PAIR : j * 256 + (p + 1) * PAIR]
                r, k, v, dp, ep = (col(j) for j in range(5))
                db = db_ref[rows, :]
                db = jnp.where(lane_lo, db[:, 2 * p : 2 * p + 1], db[:, 2 * p + 1 : 2 * p + 2])
                ld = -0.6065306597126334 / (1.0 + jnp.exp(-(dp + db)))
                er = 1.0 / (1.0 + jnp.exp(-(ep + eb_ref[:, lanes])))
                u = k * lax.rsqrt(head_sums(k * k, mask) + 1e-06)
                self_ref[rows, lanes] = head_sums(r * k * st_ref[:, lanes], mask) * v
                hi, lo = split2(ld)
                cum = mm(tril, hi) + mm(tril, lo)
                end = cum[CHUNK - 1 : CHUNK, :]
                eci = jnp.exp(-cum)
                a = (-u * jnp.exp(cum - ld)).astype(BF)
                ri = r * jnp.exp(cum)
                ue = u * er
                b = (ue * eci).astype(BF)
                ko = (k * eci).astype(BF)
                tail = jnp.exp(end - cum)
                bt = (ue * tail).astype(BF)
                kt = (k * tail).astype(BF)
                ar = jnp.concatenate([a, ri.astype(BF)], axis=0)
                m13 = mm_t(ar, block_diag(b, mask))
                m24 = mm_t(ar, block_diag(ko, mask))
                m1 = jnp.where(strict, m13[:CHUNK], 0.0)
                m3 = jnp.where(causal, m13[CHUNK:], 0.0).astype(BF)
                m24 = jnp.concatenate(
                    [jnp.where(strict, m24[:CHUNK], 0.0), jnp.where(causal, m24[CHUNK:], 0.0)], axis=0
                ).astype(BF)
                vb = v.astype(BF)
                mv = mm(m24, block_diag(vb, mask))
                x = eye + jnp.where((t_i // 2) == (s_i // 2), m1, 0.0)
                units.append(
                    dict(rows=rows, lanes=lanes, p=p, r0=r0, a=a, ri=ri, m1=m1, m3=m3, mv=mv, x=x,
                         bt=bt, kt=kt, vb=vb, end=end)
                )
        size = 2
        while size < CHUNK:
            corner = ((t_i // (2 * size)) == (s_i // (2 * size))) & ((t_i // size) != (s_i // size))
            for n in units:
                xb = n["x"].astype(BF)
                n["xb"] = xb
                c = jnp.where(corner, n["m1"], 0.0).astype(BF)
                n["y"] = mm(xb, block_diag(c, mask)).astype(BF)
            for n in units:
                n["x"] = n["x"] + mm(n["y"], block_diag(n["xb"], mask))
            size *= 2
        for n in units:
            right = jnp.concatenate(
                [block_diag(n["a"], mask), block_diag(n["mv"][:CHUNK].astype(BF), mask)], axis=1
            )
            n["pq"] = mm(n["x"].astype(BF), right).astype(BF)
        for n in units:
            pb, qb = n["pq"][:, :PAIR], n["pq"][:, PAIR:]
            m3pq = mm(n["m3"], jnp.concatenate([block_diag(pb, mask), block_diag(qb, mask)], axis=1))
            r_s[n["rows"], n["lanes"]] = (n["ri"] + m3pq[:, :PAIR]).astype(BF)
            out_ref[n["rows"], n["lanes"]] = m3pq[:, PAIR:] + n["mv"][CHUNK:]
            big = pl.ds(pl.multiple_of(n["r0"] * 2, PAIR), PAIR)
            e_s[big, n["lanes"]] = (mm_tn(pb, n["bt"]) * mask).astype(BF)
            left = jnp.concatenate([qb, n["vb"]], axis=0)
            right = jnp.concatenate([n["bt"], n["kt"]], axis=0)
            l_s[big, n["lanes"]] = mm_tn(left, right) * mask
            small = pl.ds(pl.multiple_of(n["r0"] // 8, 8), 8)
            d_s[small, n["lanes"]] = jnp.broadcast_to(jnp.exp(n["end"]), (8, PAIR))
        return carry

    lax.fori_loop(0, n_chunks // group, do_group, 0)

    eye2 = (iota((PAIR, PAIR), 0) == iota((PAIR, PAIR), 1)).astype(F32)
    state = [jnp.concatenate([jnp.zeros((PAIR, PAIR), F32), eye2], axis=0) for _ in range(2)]
    for c in range(n_chunks):
        rows = slice(c * CHUNK, (c + 1) * CHUNK)
        big = slice(c * PAIR, (c + 1) * PAIR)
        for p in range(2):
            lanes = slice(p * PAIR, (p + 1) * PAIR)
            sb = state[p].astype(BF)
            o = mm_t(r_s[rows, lanes], sb)
            out_ref[rows, lanes] = out_ref[rows, lanes] + o[:, :PAIR]
            rt_ref[rows, lanes] = o[:, PAIR:].astype(BF)
            decayed = state[p] * d_s[c * 8 : c * 8 + 1, lanes]
            moved = mm(sb, e_s[big, lanes])
            state[p] = decayed + moved
            state[p] = jnp.concatenate([state[p][:PAIR] + l_s[big, lanes], state[p][PAIR:]], axis=0)
    for p in range(2):
        lanes = slice(p * PAIR, (p + 1) * PAIR)
        tl_ref[0:64, lanes] = (state[p][PAIR : PAIR + 64] + state[p][PAIR + 64 :]).astype(BF)
        tl_ref[64:128, lanes] = (state[p][0:64] + state[p][64:128]).astype(BF)


def state_kernel(tl_ref, enter_ref, cbuf, ysend, ybuf, zsend, zbuf, cs, cr, ys, yr, zs, zr):
    z, y, c = lax.axis_index("ep_0"), lax.axis_index("ep_1"), lax.axis_index("ep_2")
    barrier = pltpu.get_barrier_semaphore()
    pl.semaphore_signal(barrier, inc=1, device_id={"ep_2": 1 - c}, device_id_type=MESH)
    for d in range(1, 4):
        pl.semaphore_signal(barrier, inc=1, device_id={"ep_1": (y + d) % 4}, device_id_type=MESH)
        pl.semaphore_signal(barrier, inc=1, device_id={"ep_0": (z + d) % 4}, device_id_type=MESH)
    pl.semaphore_wait(barrier, 7)
    mask = pair_mask().astype(F32).astype(BF)

    def times(left, t):
        return jnp.concatenate(
            [mm(left[:, q * PAIR : (q + 1) * PAIR].astype(BF),
                block_diag(t[:, q * PAIR : (q + 1) * PAIR].astype(BF), mask)) for q in range(2)],
            axis=1,
        )

    def compose(early, late):
        joined = times(early, late[:64])
        return jnp.concatenate([joined[:64], joined[64:] + late[64:]], axis=0)

    cp = pltpu.make_async_remote_copy(
        src_ref=tl_ref, dst_ref=cbuf, send_sem=cs, recv_sem=cr,
        device_id={"ep_2": 1 - c}, device_id_type=MESH)
    cp.start()
    cp.wait()
    mine = tl_ref[...].astype(F32)
    other = cbuf[...].astype(F32)
    first = jnp.where(c == 0, mine, other)
    second = jnp.where(c == 0, other, mine)

    def exchange(value, send, buf, ss, rs, axis, me):
        send[...] = value.astype(BF)
        copies = []
        for d in range(1, 4):
            cp = pltpu.make_async_remote_copy(
                src_ref=send, dst_ref=buf.at[d], send_sem=ss.at[d], recv_sem=rs.at[d],
                device_id={axis: (me + d) % 4}, device_id_type=MESH)
            cp.start()
            copies.append(cp)
        buf[0] = value.astype(BF)
        for cp in copies:
            cp.wait()

    exchange(compose(first, second), ysend, ybuf, ys, yr, "ep_1", y)
    run = ybuf[y % 4].astype(F32)
    ident = (iota((64, 256), 0) == iota((64, 256), 1) % 64).astype(F32)
    before = jnp.concatenate([ident, jnp.zeros((64, 256), F32)], axis=0)
    for j in range(1, 4):
        before = jnp.where(y == j, run, before)
        run = compose(run, ybuf[(y - j + 4) % 4].astype(F32))
    exchange(run, zsend, zbuf, zs, zr, "ep_0", z)
    state = jnp.zeros((64, 256), F32)
    enter = state
    for j in range(0, 3):
        piece = zbuf[(z - j + 4) % 4].astype(F32)
        state = (times(state, piece[:64]) if j else 0.0) + piece[64:]
        enter = jnp.where(z == j + 1, state, enter)
    enter = times(enter, before[:64]) + before[64:]
    enter = jnp.where(c == 0, enter, times(enter, first[:64]) + first[64:])
    enter_ref[...] = enter.astype(BF)


def finish_kernel(out_ref, rt_ref, self_ref, enter_ref, gain_ref, w_ref, part_ref, heads):
    mask = pair_mask().astype(F32).astype(BF)
    for p in range(2):
        lanes = slice(p * PAIR, (p + 1) * PAIR)
        ent = block_diag(enter_ref[:, lanes], mask)
        o = out_ref[:, lanes] + mm_t(rt_ref[:, lanes], ent)
        o = o - head_sums(o, mask) * (1.0 / 64)
        var = head_sums(o * o, mask) * (1.0 / 64)
        h = o * lax.rsqrt(var + 0.00064) * gain_ref[:, lanes] + self_ref[:, lanes]
        heads[:, lanes] = h.astype(BF)
    for j in range(4):
        cols = slice(j * 512, (j + 1) * 512)
        part_ref[:, cols] = mm(heads[...], w_ref[:, cols]).astype(BF)


def vspec(n):
    return [pl.BlockSpec(memory_space=VMEM)] * n


def copy_for_each(value, axis):
    copies = jnp.broadcast_to(value, (lax.axis_size(axis), *value.shape))
    return lax.all_to_all(copies, axis, split_axis=0, concat_axis=0, tiled=True)


def rms_rows(values, feature_gain):
    wide_values = values.astype(F32)
    inverse = lax.rsqrt(jnp.mean(wide_values * wide_values, axis=1, keepdims=True) + 1e-06)
    return (wide_values * inverse * feature_gain).astype(BF)


def per_device(
    mixer_input_rows, mixer_norm_scale, decay_bias_table, erase_bias_table,
    receive_weight, key_weight, value_weight, decay_weight, erase_weight,
    self_token_scale, head_norm_scale, output_weight,
    expert_input_rows, expert_norm_scale, routes, router_weights,
    routed_gate_weight, routed_up_weight, routed_down_weight,
    common_gate_weight, common_up_weight, common_down_weight,
):
    normed_a = rms_rows(mixer_input_rows, mixer_norm_scale)
    row_piece = copy_for_each(normed_a, "tp").reshape(512, -1)

    normed_b = rms_rows(expert_input_rows, expert_norm_scale)
    route_weight = 2.5 * router_weights / jnp.sum(router_weights, axis=1, keepdims=True)
    token_count, top_count = routes.shape
    expert_count = lax.axis_size(EP) * lax.axis_size("tp")
    capacity = 2 * token_count * top_count // expert_count
    slots = expert_count * capacity
    chosen = routes.reshape(-1)
    onehot = (chosen[:, None] == jnp.arange(expert_count, dtype=jnp.int32)[None, :]).astype(BF)
    pairs = token_count * top_count
    lower = (jnp.arange(pairs)[:, None] > jnp.arange(pairs)[None, :]).astype(BF)
    counts = jnp.dot(lower, onehot, preferred_element_type=F32)
    rank = jnp.sum(counts * onehot, axis=1).astype(jnp.int32)
    slot_index = (chosen * capacity + rank).reshape(token_count, top_count)
    slot_ids = jnp.arange(slots, dtype=jnp.int32)[None, :]
    hit0 = slot_index[:, 0:1] == slot_ids
    hit1 = slot_index[:, 1:2] == slot_ids
    place = (hit0 | hit1).astype(BF)
    outgoing = lax.dot_general(place, normed_b, (((0,), (0,)), ((), ())), preferred_element_type=F32)
    outgoing = outgoing.astype(BF).reshape(expert_count, capacity, -1)
    arrived = lax.all_to_all(outgoing, EP_TP, split_axis=0, concat_axis=0, tiled=True)
    flat_rows = arrived.reshape(slots, -1)

    eb = jnp.repeat(erase_bias_table, 64).reshape(1, 256)
    out_l, rt, selft, tl = pl.pallas_call(
        mixer_kernel,
        out_shape=(
            jax.ShapeDtypeStruct((512, 256), F32),
            jax.ShapeDtypeStruct((512, 256), BF),
            jax.ShapeDtypeStruct((512, 256), F32),
            jax.ShapeDtypeStruct((128, 256), BF),
        ),
        in_specs=vspec(9),
        out_specs=tuple(vspec(4)),
        scratch_shapes=[
            VMEM((512, 1280), F32),
            VMEM((512, 256), BF),
            VMEM((1024, 256), BF),
            VMEM((1024, 256), F32),
            VMEM((64, 256), F32),
        ],
        cost_estimate=pl.CostEstimate(flops=6_000_000_000, bytes_accessed=10_000_000, transcendentals=0),
        name="mixer_local",
    )(row_piece, receive_weight, key_weight, value_weight, decay_weight, erase_weight,
      decay_bias_table, eb, self_token_scale.reshape(1, 256))

    enter = pl.pallas_call(
        state_kernel,
        out_shape=jax.ShapeDtypeStruct((64, 256), BF),
        in_specs=vspec(1),
        out_specs=vspec(1)[0],
        scratch_shapes=[
            VMEM((128, 256), BF),
            VMEM((128, 256), BF),
            VMEM((4, 128, 256), BF),
            VMEM((128, 256), BF),
            VMEM((4, 128, 256), BF),
            pltpu.SemaphoreType.DMA, pltpu.SemaphoreType.DMA,
            pltpu.SemaphoreType.DMA((4,)), pltpu.SemaphoreType.DMA((4,)),
            pltpu.SemaphoreType.DMA((4,)), pltpu.SemaphoreType.DMA((4,)),
        ],
        compiler_params=pltpu.CompilerParams(collective_id=0, has_side_effects=True),
        cost_estimate=pl.CostEstimate(flops=4_000_000_000, bytes_accessed=1_000_000, transcendentals=0),
        name="state_exchange",
    )(tl)

    partial = pl.pallas_call(
        finish_kernel,
        out_shape=jax.ShapeDtypeStruct((512, 2048), BF),
        in_specs=vspec(6),
        out_specs=vspec(1)[0],
        scratch_shapes=[VMEM((512, 256), BF)],
        cost_estimate=pl.CostEstimate(flops=2_000_000_000, bytes_accessed=4_000_000, transcendentals=0),
        name="mixer_finish",
    )(out_l, rt, selft, enter, head_norm_scale.reshape(1, 256), output_weight)
    pieces = lax.all_to_all(partial.reshape(4, 128, 2048), "tp", split_axis=0, concat_axis=0, tiled=True)
    mixer_output = pieces.astype(F32).sum(axis=0).astype(BF)

    gate_part, up_part, down_part = routed_gate_weight[0], routed_up_weight[0], routed_down_weight[0]
    expert_hidden = (
        jax.nn.silu(jnp.dot(flat_rows, gate_part, preferred_element_type=F32))
        * jnp.dot(flat_rows, up_part, preferred_element_type=F32)
    ).astype(BF)
    result = jnp.dot(expert_hidden, down_part, preferred_element_type=F32).astype(BF)
    returned = lax.all_to_all(
        result.reshape(expert_count, capacity, -1), EP_TP, split_axis=0, concat_axis=0, tiled=True
    )
    back_rows = returned.reshape(slots, -1)
    weights = jnp.where(hit0, route_weight[:, 0:1], 0.0) + jnp.where(hit1, route_weight[:, 1:2], 0.0)
    whi, wlo = split2(weights)
    routed = jnp.dot(whi, back_rows, preferred_element_type=F32) + jnp.dot(
        wlo, back_rows, preferred_element_type=F32
    )
    shared_hidden = (
        jax.nn.silu(jnp.dot(normed_b, common_gate_weight, preferred_element_type=F32))
        * jnp.dot(normed_b, common_up_weight, preferred_element_type=F32)
    ).astype(BF)
    shared_term = jnp.dot(shared_hidden, common_down_weight, preferred_element_type=F32)
    mixed_b = (routed + shared_term).astype(BF)
    return (mixer_output, mixed_b)


def solution(mesh):
    split = Mesh(mesh.devices.reshape(4, 4, 2, mesh.shape["tp"]), ("ep_0", "ep_1", "ep_2", "tp"))
    in_specs = (
        P(EP_TP, None), P(), P(EP, "tp"), P("tp"),
        P(None, "tp"), P(None, "tp"), P(None, "tp"), P(None, "tp"), P(None, "tp"),
        P("tp", None), P("tp"), P("tp", None),
        P(EP_TP, None), P(), P(EP_TP, None), P(EP_TP, None),
        P(EP_TP, None, None), P(EP_TP, None, None), P(EP_TP, None, None),
        P(), P(), P(),
    )
    out_specs = (P(EP_TP, None), P(EP_TP, None))
    return jax.shard_map(
        per_device, mesh=split, in_specs=in_specs, out_specs=out_specs, check_vma=False
    )
```

time: 486 us -> 161 us (0.33)
  other arithmetic: 198 us -> 5.73 us
  matrix products: 96 us -> 24 us
  local copies, waits for them, and re-layouts: 71.5 us -> 16 us
  blocking collectives: 43.8 us -> 0 us
  Pallas kernels: 0 us -> 40.2 us
  waiting for transfers between devices: 32.1 us -> 47.5 us
  starting transfers between devices: 40.1 us -> 25.9 us
    another operation x27 -> x0, other arithmetic: 165 us -> none  [the longest x16 163 us: block_pass(): jax.scipy.linalg.solve_triangular(system, right_side, lower=True, unit_di...]
    dot_general x94 -> x8, matrix products: 92.8 us -> 24 us  [the longest x1 9.97 us: per_device(): jnp.dot(expert_hidden, down_part, preferred_element_type=F32).astype(BF)]
    all_gather x6 -> x0, blocking collectives: 43.8 us -> none  [entering_2(): lax.all_gather(part.astype(kind), axis)]
    pallas_call x0 -> x3, Pallas kernels: none -> 40.2 us  [the longest x1 20.1 us: per_device(): pl.pallas_call(state_kernel, out_shape=jax.ShapeDtypeStruct((64, 256), BF...]
    another operation x12 -> x1, local copies, waits for them, and re-layouts: 22.9 us -> 0.68 us  [per_device(): eb = jnp.repeat(erase_bias_table, 64).reshape(1, 256)]
    mul x19 -> x0, other arithmetic: 20.1 us -> none  [the longest x8 8.06 us: block_pass(): erase_in = -unit_key * jnp.exp(cumulative - log_decay)]
    all_to_all x1, waiting for transfers between devices: 5.08 us -> 20.8 us  [copy_for_each(): return lax.all_to_all(copies, axis, split_axis=0, concat_axis=0, tiled=True)]
    squeeze x16 -> x0, local copies, waits for them, and re-layouts: 14.1 us -> none  [local_states(): lax.scan(block_pass, start_state, tuple((blocked(member) for member in me...]
  transfers between devices with their start and end apart: 4 -> 4, of which waited for: 2 -> 3; matrix products, arithmetic and copies ran while one was open for 71% -> 23% of each run, Pallas kernels for 0% -> 25%
where the time goes in v1:
time: 161 us; the launch traced here: 160 us
  waiting for transfers between devices  47.5 us (30%)
  Pallas kernels  40.2 us (25%)
  starting transfers between devices  25.9 us (16%)
  matrix products  24 us (15%)
  local copies, waits for them, and re-layouts  16 us (10%)
  other arithmetic  5.73 us (4%)
    all_to_all x1, waiting for transfers between devices, per_device(): lax.all_to_all(result.reshape(expert_count, capacity, -1), EP_TP, split_a...  24.1 us
    all_to_all x1, waiting for transfers between devices, copy_for_each(): return lax.all_to_all(copies, axis, split_axis=0, concat_axis=0, tiled=True)  20.8 us
    pallas_call x1, Pallas kernels, per_device(): pl.pallas_call(state_kernel, out_shape=jax.ShapeDtypeStruct((64, 256), BF...  20.1 us
    pallas_call x1, Pallas kernels, per_device(): pl.pallas_call(mixer_kernel, out_shape=(jax.ShapeDtypeStruct((512, 256),...  15.6 us
    all_to_all x1, starting transfers between devices, per_device(): lax.all_to_all(outgoing, EP_TP, split_axis=0, concat_axis=0, tiled=True)  10 us
    dot_general x1, matrix products, per_device(): jnp.dot(expert_hidden, down_part, preferred_element_type=F32).astype(BF)  9.97 us
    dot_general x1, matrix products, per_device(): jnp.dot(flat_rows, gate_part, preferred_element_type=F32)  6.62 us
    all_to_all x1, starting transfers between devices, per_device(): lax.all_to_all(result.reshape(expert_count, capacity, -1), EP_TP, split_a...  6.33 us
  transfers between devices with their start and end apart: 4, of which 3 were waited for; matrix products, arithmetic and copies ran while one was open for 23% of the time, Pallas kernels for 25%

profile of v1, /device:TPU:1, one launch (start us, length us, event | category | flops | bytes accessed | tf_op | source)
XLA Modules:
  0.0 160.2 jit_solution(11696015710974753659)
XLA Ops:
  0.6 1.3 fusion.16
  2.0 1.2 fusion.18
  3.2 1.6 broadcast_in_dim.37
  4.8 5.0 %all-to-all-start = ((bf16[4,128,2048]{2,1,0:T(8,128)(2,1)}), bf16[4,128,2048]{2,1,0:T(8,128)(2,1)}, u32[]{:S(2)}, u32[]{:S(2)}) async-start(bf16[4,128,2048]{2,1,0:T(8,128)(2,1)} %broadcast_in_dim.37), calls=%async_computation | async-start | bytes 4194304 | tf_op jit(solution)/shard_map/all_to_all | solution.py:256
  9.9 0.1 eq.45
  10.0 0.2 fusion.14
  10.5 0.2 fusion.19
  10.7 1.9 %convolution_convert_fusion = bf16[512,2048]{1,0:T(8,128)(2,1)S(1)} fusion(s32[128]{0:T(128)S(1)} %get-tuple-element.13, s32[128]{0:T(128)S(1)} %get-tuple-element.12, bf16[128,2048]{1,0:T(8,128)(2,1)} %param.34, f32[2048]{0:T(1024)S(1)} %copy-done.6, f32[128]{0:T(128)S(1)} %add_rsqrt_fusion), kind=kOutput, calls=%fused_computation.7 | convolution fusion | flops 270729216 | bytes 2631168 | tf_op jit(solution)/shard_map/dot_general | solution.py:293
  12.6 2.2 %reshape.56 = bf16[128,4,2048]{2,1,0:T(4,128)(2,1)} reshape(bf16[512,2048]{1,0:T(8,128)(2,1)S(1)} %convolution_convert_fusion) | data formatting | bytes 4194304 | tf_op jit(solution)/shard_map/reshape | solution.py:294
  14.9 20.8 %all-to-all-done = bf16[4,128,2048]{2,1,0:T(8,128)(2,1)} async-done(((bf16[4,128,2048]{2,1,0:T(8,128)(2,1)}), bf16[4,128,2048]{2,1,0:T(8,128)(2,1)}, u32[]{:S(2)}, u32[]{:S(2)}) %all-to-all-start) | async-done | bytes 2097184 | tf_op jit(solution)/shard_map/all_to_all | solution.py:256
  35.7 10.0 %all-to-all-start.2 = ((bf16[128,4,2048]{2,1,0:T(4,128)(2,1)}), bf16[128,4,2048]{2,1,0:T(4,128)(2,1)S(1)}, u32[]{:S(2)}, u32[]{:S(2)}) async-start(bf16[128,4,2048]{2,1,0:T(4,128)(2,1)} %reshape.56), calls=%async_computation.2 | async-start | bytes 4194304 | tf_op jit(solution)/shard_map/all_to_all | solution.py:295
  45.7 0.9 copy.33.db_ref
  46.7 0.7 reshape_reshape.3.eb_ref
  47.4 0.6 reshape.53.st_ref
  48.0 15.6 %mixer_local.1 = (f32[512,256]{1,0:T(8,128)}, bf16[512,256]{1,0:T(8,128)(2,1)}, f32[512,256]{1,0:T(8,128)}, bf16[128,256]{1,0:T(8,128)(2,1)}) custom-call(bf16[512,2048]{1,0:T(8,128)(2,1)} %bitcast.rows_ref, bf16[2048,256]{1,0:T(8,128)(2,1)} %wr_ref.1, bf16[2048,256]{1,0:T(8,128)(2,1)} %wk_ref.1, bf16[2048,256]{1,0:T(8,128)(2,1)} %wv_ref.1, ...), custom_call_target="tpu_custom_call" | custom-call | flops 6000000000 | bytes 10000000 | tf_op jit(solution)/shard_map/mixer_local/pallas_call | solution.py:299
  63.6 20.1 %state_exchange.1.enter_ref = bf16[64,256]{1,0:T(8,128)(2,1)} custom-call(bf16[128,256]{1,0:T(8,128)(2,1)} %get-tuple-element.9.tl_ref), custom_call_target="tpu_custom_call" | custom-call | flops 4000000000 | bytes 1000000 | tf_op jit(solution)/shard_map/state_exchange/pallas_call | solution.py:321
  83.7 4.5 %mixer_finish.1 = bf16[512,2048]{1,0:T(8,128)(2,1)} custom-call(f32[512,256]{1,0:T(8,128)} %get-tuple-element.6.out_ref, bf16[512,256]{1,0:T(8,128)(2,1)} %get-tuple-element.7.rt_ref, f32[512,256]{1,0:T(8,128)} %get-tuple-element.8.self_ref, bf16[64,256]{1,0:T(8,128)(2,1)} %state_exchange.1.enter_ref, f32[1,256]{1,0:T(1,128)} %bitcast.34, ...), custom_call_target="tpu_custom_call" | custom-call | flops 2000000000 | bytes 4000000 | tf_op jit(solution)/shard_map/mixer_finish/pallas_call | solution.py:341
  88.2 4.6 %all-to-all-start.1 = ((bf16[4,128,2048]{2,1,0:T(8,128)(2,1)}), bf16[4,128,2048]{2,1,0:T(8,128)(2,1)}, u32[]{:S(2)}, u32[]{:S(2)}) async-start(bf16[4,128,2048]{2,1,0:T(8,128)(2,1)} %bitcast.33), calls=%async_computation.1 | async-start | bytes 4194304 | tf_op jit(solution)/shard_map/all_to_all | solution.py:350
  92.9 2.1 %reshape.57 = bf16[512,2048]{1,0:T(8,128)(2,1)} reshape(bf16[128,4,2048]{2,1,0:T(4,128)(2,1)S(1)} %all-to-all-done.2) | data formatting | bytes 4194304 | tf_op jit(solution)/shard_map/reshape | solution.py:296
  95.0 6.6 %fusion.4 = f32[512,1024]{1,0:T(8,128)} fusion(bf16[512,2048]{1,0:T(8,128)(2,1)} %reshape.57, bf16[1,2048,1024]{2,1,0:T(8,128)(2,1)} %param.38), kind=kOutput, calls=%fused_computation.4 | convolution fusion | flops 2147483648 | bytes 8388608 | tf_op jit(solution)/shard_map/dot_general | solution.py:355
  101.6 10.0 %fusion.6 = bf16[512,2048]{1,0:T(8,128)(2,1)} fusion(bf16[1,1024,2048]{2,1,0:T(8,128)(2,1)} %param.40, f32[512,1024]{1,0:T(8,128)} %fusion.4, bf16[512,2048]{1,0:T(8,128)(2,1)S(1)} %copy-done.4, bf16[1,2048,1024]{2,1,0:T(8,128)(2,1)} %param.39), kind=kOutput, calls=%fused_computation.6 | convolution fusion | flops 4299161600 | bytes 14680064 | tf_op jit(solution)/shard_map/dot_general | solution.py:358
  111.6 4.1 %reshape.58 = bf16[128,4,2048]{2,1,0:T(4,128)(2,1)} reshape(bf16[512,2048]{1,0:T(8,128)(2,1)} %fusion.6) | data formatting | bytes 4194304 | tf_op jit(solution)/shard_map/reshape | solution.py:360
  115.7 2.5 %all-to-all-done.1 = bf16[4,128,2048]{2,1,0:T(8,128)(2,1)} async-done(((bf16[4,128,2048]{2,1,0:T(8,128)(2,1)}), bf16[4,128,2048]{2,1,0:T(8,128)(2,1)}, u32[]{:S(2)}, u32[]{:S(2)}) %all-to-all-start.1) | async-done | bytes 2097184 | tf_op jit(solution)/shard_map/all_to_all | solution.py:350
  118.2 6.3 %all-to-all-start.3 = ((bf16[128,4,2048]{2,1,0:T(4,128)(2,1)}), bf16[128,4,2048]{2,1,0:T(4,128)(2,1)}, u32[]{:S(2)}, u32[]{:S(2)}) async-start(bf16[128,4,2048]{2,1,0:T(4,128)(2,1)} %reshape.58), calls=%async_computation.3 | async-start | bytes 4194304 | tf_op jit(solution)/shard_map/all_to_all | solution.py:359
  124.6 1.6 fusion.51
  126.2 1.8 %fusion.15 = f32[128,2048]{1,0:T(8,128)} fusion(bf16[256,2048]{1,0:T(8,128)(2,1)S(1)} %copy-done, bf16[2048,256]{1,0:T(8,128)(2,1)S(1)} %copy-done.5, f32[128,256]{1,0:T(8,128)S(1)} %fusion.51, bf16[128,2048]{1,0:T(8,128)(2,1)S(1)} %copy-done.2, f32[2048]{0:T(1024)S(1)} %copy-done.6, f32[128]{0:T(128)S(1)} %add_rsqrt_fusion), kind=kOutput, calls=%fused_computation.20 | convolution fusion | flops 269680640 | bytes 3809792 | tf_op jit(solution)/shard_map/dot_general | solution.py:372
  128.0 2.9 %reduce_sum.49 = bf16[128,2048]{1,0:T(8,128)(2,1)} reduce(bf16[4,128,2048]{2,1,0:T(8,128)(2,1)} %all-to-all-done.1, bf16[]{:T(256)} %constant.15.clone.1), dimensions={0}, to_apply=%region_1.0 | reduce | flops 786432 | bytes 2621442 | tf_op jit(solution)/shard_map/reduce_sum | solution.py:351
  131.0 24.1 %all-to-all-done.3 = bf16[128,4,2048]{2,1,0:T(4,128)(2,1)} async-done(((bf16[128,4,2048]{2,1,0:T(4,128)(2,1)}), bf16[128,4,2048]{2,1,0:T(4,128)(2,1)}, u32[]{:S(2)}, u32[]{:S(2)}) %all-to-all-start.3) | async-done | bytes 2097184 | tf_op jit(solution)/shard_map/all_to_all | solution.py:359
  155.1 2.5 %reshape.59 = bf16[512,2048]{1,0:T(8,128)(2,1)S(1)} reshape(bf16[128,4,2048]{2,1,0:T(4,128)(2,1)} %all-to-all-done.3) | data formatting | bytes 4194304 | tf_op jit(solution)/shard_map/reshape | solution.py:362
  157.6 0.5 fusion.41
  158.2 0.7 copy-done.3
  158.9 1.4 fusion.10
  (36 shorter events, 0.5 us)
Async XLA Ops:
  0.6 125.6 %copy-start = (bf16[256,2048]{1,0:T(8,128)(2,1)S(1)}, bf16[256,2048]{1,0:T(8,128)(2,1)}, u32[]{:S(2)}) copy-start(bf16[256,2048]{1,0:T(8,128)(2,1)} %param.43) | copy-start | bytes 3145732
  4.8 5.0 %copy-start.8 = (s32[128,2]{0,1:T(2,128)S(1)}, s32[128,2]{0,1:T(2,128)}, u32[]{:S(2)}) copy-start(s32[128,2]{0,1:T(2,128)} %param.36) | copy-start | bytes 3076
  4.8 5.7 %copy-start.1 = (bf16[128,2048]{1,0:T(8,128)(2,1)S(1)}, bf16[128,2048]{1,0:T(8,128)(2,1)}, u32[]{:S(2)}) copy-start(bf16[128,2048]{1,0:T(8,128)(2,1)} %param.34) | copy-start | bytes 1572868
  4.8 5.9 %copy-start.6 = (f32[2048]{0:T(1024)S(1)}, f32[2048]{0:T(1024)}, u32[]{:S(2)}) copy-start(f32[2048]{0:T(1024)} %param.35) | copy-start | bytes 24580
  4.8 30.9 %all-to-all-start = ((bf16[4,128,2048]{2,1,0:T(8,128)(2,1)}), bf16[4,128,2048]{2,1,0:T(8,128)(2,1)}, u32[]{:S(2)}, u32[]{:S(2)}) async-start(bf16[4,128,2048]{2,1,0:T(8,128)(2,1)} %broadcast_in_dim.37), calls=%async_computation | async-start | bytes 4194304 | tf_op jit(solution)/shard_map/all_to_all | solution.py:256
  14.9 30.8 %copy-start.7 = (f32[512,4]{0,1:T(4,128)S(1)}, f32[512,4]{0,1:T(4,128)}, u32[]{:S(2)}) copy-start(f32[512,4]{0,1:T(4,128)} %param.24) | copy-start | bytes 24580
  14.9 31.7 %copy-start.11 = (f32[4]{0:T(128)S(1)}, f32[4]{0:T(128)}, u32[]{:S(2)}) copy-start(f32[4]{0:T(128)} %param.25) | copy-start | bytes 52
  14.9 32.5 %copy-start.10 = (f32[4,64]{1,0:T(4,128)S(1)}, f32[4,64]{1,0:T(4,128)}, u32[]{:S(2)}) copy-start(f32[4,64]{1,0:T(4,128)} %param.31) | copy-start | bytes 3076
  35.7 52.6 %all-to-all-start.2 = ((bf16[128,4,2048]{2,1,0:T(4,128)(2,1)}), bf16[128,4,2048]{2,1,0:T(4,128)(2,1)S(1)}, u32[]{:S(2)}, u32[]{:S(2)}) async-start(bf16[128,4,2048]{2,1,0:T(4,128)(2,1)} %reshape.56), calls=%async_computation.2 | async-start | bytes 4194304 | tf_op jit(solution)/shard_map/all_to_all | solution.py:295
  88.2 30.0 %all-to-all-start.1 = ((bf16[4,128,2048]{2,1,0:T(8,128)(2,1)}), bf16[4,128,2048]{2,1,0:T(8,128)(2,1)}, u32[]{:S(2)}, u32[]{:S(2)}) async-start(bf16[4,128,2048]{2,1,0:T(8,128)(2,1)} %bitcast.33), calls=%async_computation.1 | async-start | bytes 4194304 | tf_op jit(solution)/shard_map/all_to_all | solution.py:350
  95.0 6.6 %copy-start.4 = (bf16[512,2048]{1,0:T(8,128)(2,1)S(1)}, bf16[512,2048]{1,0:T(8,128)(2,1)}, u32[]{:S(2)}) copy-start(bf16[512,2048]{1,0:T(8,128)(2,1)} %reshape.57) | copy-start | bytes 6291460
  115.7 8.9 %copy-start.9 = (f32[128,2]{0,1:T(2,128)S(1)}, f32[128,2]{0,1:T(2,128)}, u32[]{:S(2)}) copy-start(f32[128,2]{0,1:T(2,128)} %param.37) | copy-start | bytes 3076
  115.7 8.9 %copy-start.2 = (bf16[128,2048]{1,0:T(8,128)(2,1)S(1)}, bf16[128,2048]{1,0:T(8,128)(2,1)}, u32[]{:S(2)}) copy-start(bf16[128,2048]{1,0:T(8,128)(2,1)} %param.34) | copy-start | bytes 1572868
  115.7 10.5 %copy-start.5 = (bf16[2048,256]{1,0:T(8,128)(2,1)S(1)}, bf16[2048,256]{1,0:T(8,128)(2,1)}, u32[]{:S(2)}) copy-start(bf16[2048,256]{1,0:T(8,128)(2,1)} %param.42) | copy-start | bytes 3145732
  118.2 36.9 %all-to-all-start.3 = ((bf16[128,4,2048]{2,1,0:T(4,128)(2,1)}), bf16[128,4,2048]{2,1,0:T(4,128)(2,1)}, u32[]{:S(2)}, u32[]{:S(2)}) async-start(bf16[128,4,2048]{2,1,0:T(4,128)(2,1)} %reshape.58), calls=%async_computation.3 | async-start | bytes 4194304 | tf_op jit(solution)/shard_map/all_to_all | solution.py:359
  157.6 1.2 copy-start.3

commit v2 on v1

--- a/solution.py
+++ b/solution.py
@@ -54,17 +54,15 @@
 
 
 def mixer_kernel(
-    rows_ref, wr_ref, wk_ref, wv_ref, wd_ref, we_ref, db_ref, eb_ref, st_ref,
+    pr_ref, db_ref, eb_ref, st_ref, after_ref,
     out_ref, rt_ref, self_ref, tl_ref,
-    pr_ref, r_s, e_s, l_s, d_s,
+    r_s, e_s, l_s, d_s,
 ):
-    n_rows = rows_ref.shape[0]
+    n_rows = pr_ref.shape[0]
     n_chunks = n_rows // CHUNK
     group = 4
     mask_b = pair_mask()
     mask = mask_b.astype(F32).astype(BF)
-    for j, w in enumerate((wr_ref, wk_ref, wv_ref, wd_ref, we_ref)):
-        pr_ref[:, j * 256 : (j + 1) * 256] = mm(rows_ref[...], w[...])
 
     t_i = iota((CHUNK, PAIR), 0)
     s_i = iota((CHUNK, PAIR), 1) % 64
@@ -232,7 +230,16 @@
     enter_ref[...] = enter.astype(BF)
 
 
-def finish_kernel(out_ref, rt_ref, self_ref, enter_ref, gain_ref, w_ref, part_ref, heads):
+def finish_kernel(
+    out_ref, rt_ref, self_ref, enter_ref, gain_ref, w_hbm, res_ref,
+    heads, landed, w_s, w_sem, ss, rs,
+):
+    t = lax.axis_index("tp")
+    load = pltpu.make_async_copy(w_hbm, w_s, w_sem)
+    load.start()
+    barrier = pltpu.get_barrier_semaphore()
+    for d in range(1, 4):
+        pl.semaphore_signal(barrier, inc=1, device_id={"tp": (t + d) % 4}, device_id_type=MESH)
     mask = pair_mask().astype(F32).astype(BF)
     for p in range(2):
         lanes = slice(p * PAIR, (p + 1) * PAIR)
@@ -242,24 +249,231 @@
         var = head_sums(o * o, mask) * (1.0 / 64)
         h = o * lax.rsqrt(var + 0.00064) * gain_ref[:, lanes] + self_ref[:, lanes]
         heads[:, lanes] = h.astype(BF)
+    pl.semaphore_wait(barrier, 3)
+    copies = []
+    for d in (2, 1, 3):
+        peer = (t + d) % 4
+        cp = pltpu.make_async_remote_copy(
+            src_ref=heads.at[pl.ds(pl.multiple_of(peer * 128, 128), 128)], dst_ref=landed.at[d],
+            send_sem=ss.at[d], recv_sem=rs.at[d], device_id={"tp": peer}, device_id_type=MESH)
+        cp.start()
+        copies.append(cp)
+    load.wait()
+    own = heads[pl.ds(pl.multiple_of(t * 128, 128), 128), :]
+    for cp in copies:
+        cp.wait()
     for j in range(4):
         cols = slice(j * 512, (j + 1) * 512)
-        part_ref[:, cols] = mm(heads[...], w_ref[:, cols]).astype(BF)
+        total = mm(own, w_s[t, :, cols])
+        for d in range(1, 4):
+            total = total + mm(landed[d], w_s[(t + 4 - d) % 4, :, cols])
+        res_ref[:, cols] = total.astype(BF)
+
+
+def prep_kernel(a_ref, ga_ref, b_ref, gb_ref, routes_ref, rw_ref, na_ref, nb_ref, msg_ref, w_ref):
+    for x_ref, g_ref, o_ref in ((a_ref, ga_ref, na_ref), (b_ref, gb_ref, nb_ref)):
+        x = x_ref[...].astype(F32)
+        inverse = lax.rsqrt(jnp.mean(x * x, axis=1, keepdims=True) + 1e-06)
+        o_ref[...] = (x * inverse * g_ref[...]).astype(BF)
+    n = 128
+    c0 = routes_ref[:, 0:1].astype(F32)
+    c1 = routes_ref[:, 1:2].astype(F32)
+    lane = iota((n, n), 1)
+    lane_f = lane.astype(F32)
+    oh0 = (c0 == lane_f).astype(F32)
+    oh1 = (c1 == lane_f).astype(F32)
+    lower = (iota((n, n), 0) > lane).astype(F32).astype(BF)
+    counts = mm(lower, (oh0 + oh1).astype(BF))
+    s0 = c0 * 4.0 + jnp.sum(counts * oh0, axis=1, keepdims=True)
+    s1 = c1 * 4.0 + jnp.sum(counts * oh1, axis=1, keepdims=True)
+    rw = rw_ref[...]
+    rw = 2.5 * rw / (rw[:, 0:1] + rw[:, 1:2])
+    slot = iota((n, 512), 1).astype(F32)
+    w = jnp.where(s0 == slot, rw[:, 0:1], 0.0) + jnp.where(s1 == slot, rw[:, 1:2], 0.0)
+    hi, lo = split2(w)
+    w_ref[0:n, :] = hi
+    w_ref[n:, :] = lo
+    turned = jnp.where(lane == 0, s0, jnp.where(lane == 1, s1, 0.0)).T
+    r0, r1 = turned[0:1, :], turned[1:2, :]
+    nb = nb_ref[...]
+    pieces = jnp.concatenate([nb[:, q * 512 : (q + 1) * 512] for q in range(4)], axis=0)
+    row = iota((256, n), 0)
+    for i in range(8):
+        ident = ((i * 16 + row // 16) * 4 + row % 4).astype(F32)
+        hit = jnp.where((r0 == ident) | (r1 == ident), 1.0, 0.0)
+        piece = (row // 4) % 4
+        oh = jnp.concatenate([jnp.where(piece == q, hit, 0.0).astype(BF) for q in range(4)], axis=1)
+        msg_ref[i * 16 : (i + 1) * 16] = mm(oh, pieces).astype(BF).reshape(16, 16, 512)
+
+
+def order_mask(back):
+    r, l = iota((256, 256), 0), iota((256, 256), 1)
+    if back:
+        r, l = l, r
+    want = ((l // 4) % 4 == r // 64) & (l // 16 == (r % 64) // 4) & (l % 4 == r % 4)
+    return want.astype(F32).astype(BF)
+
+
+def unpack_rows(msg_ref, x_ref):
+    order = order_mask(False)
+    for i in range(8):
+        rows = mm(order, msg_ref[i * 16 : (i + 1) * 16].reshape(256, 512)).astype(BF)
+        for q in range(4):
+            x_ref[i * 64 : (i + 1) * 64, q * 512 : (q + 1) * 512] = rows[q * 64 : (q + 1) * 64]
+
+
+def ring_kernel(x_ref, wr_ref, wk_ref, wv_ref, wd_ref, we_ref, pr_ref, held, ss, rs, fs, fr):
+    t = lax.axis_index("tp")
+    right, left = (t + 1) % 4, (t + 3) % 4
+    barrier = pltpu.get_barrier_semaphore()
+    for q in (left, right):
+        pl.semaphore_signal(barrier, inc=1, device_id={"tp": q}, device_id_type=MESH)
+    pl.semaphore_wait(barrier, 2)
+    n = 4
+    step = 128 // n
+    rows = lambda k: pl.ds(k * step, step)
+    own = {}
+    for i in range(n):
+        for slot, k, peer in ((0, i, right), (1, (i + n // 2) % n, left)):
+            cp = pltpu.make_async_remote_copy(
+                src_ref=x_ref.at[rows(k)], dst_ref=held.at[slot, rows(k)],
+                send_sem=ss.at[slot * n + k], recv_sem=rs.at[slot * n + k],
+                device_id={"tp": peer}, device_id_type=MESH)
+            cp.start()
+            own[slot, k] = cp
+
+    def project(block, who):
+        at = pl.ds(pl.multiple_of(who * 128, 128), 128)
+        for j, w in enumerate((wr_ref, wk_ref, wv_ref, wd_ref, we_ref)):
+            pr_ref[at, j * 256 : (j + 1) * 256] = mm(block, w[...])
+
+    project(x_ref[...], t)
+    passed = []
+    for i in range(n // 2):
+        for slot, k, peer in ((0, i, right), (1, i + n // 2, left)):
+            own[slot, k].wait_recv()
+            cp = pltpu.make_async_remote_copy(
+                src_ref=held.at[slot, rows(k)], dst_ref=held.at[2, rows(k)],
+                send_sem=fs.at[k], recv_sem=fr.at[k],
+                device_id={"tp": peer}, device_id_type=MESH)
+            cp.start()
+            passed.append(cp)
+    for i in range(n // 2):
+        own[0, i + n // 2].wait_recv()
+        own[1, i].wait_recv()
+    project(held[0], left)
+    project(held[1], right)
+    for cp in passed:
+        cp.wait()
+    project(held[2], (t + 2) % 4)
+    for cp in own.values():
+        cp.wait_send()
+
+
+def expert_kernel(
+    msg_ref, g_hbm, u_hbm, d_hbm, w_hbm, after_ref, res_ref, wall_hbm,
+    x_s, g_s, u_s, d_s, h_s, w_s, g_sem, u_sem, d_sem, w_sem, ss, rs, fs, fr, cs, cr,
+):
+    t, c = lax.axis_index("tp"), lax.axis_index("ep_2")
+    right, left = (t + 1) % 4, (t + 3) % 4
+    barrier = pltpu.get_barrier_semaphore()
+    for q in (left, right):
+        pl.semaphore_signal(barrier, inc=1, device_id={"tp": q}, device_id_type=MESH)
+    pl.semaphore_signal(barrier, inc=1, device_id={"ep_2": 1 - c}, device_id_type=MESH)
+    loads = []
+    for j in range(4):
+        for src, dst, sem in ((g_hbm, g_s, g_sem), (u_hbm, u_s, u_sem)):
+            cp = pltpu.make_async_copy(src.at[:, j * 256 : (j + 1) * 256], dst.at[j], sem.at[j])
+            cp.start()
+            loads.append(cp)
+    own_w = pltpu.make_async_copy(w_hbm, w_s, w_sem.at[0])
+    own_w.start()
+    for j in range(4):
+        pltpu.make_async_copy(d_hbm.at[:, j * 512 : (j + 1) * 512], d_s.at[j], d_sem.at[j]).start()
+    pl.semaphore_wait(barrier, 3)
+    own_w.wait()
+    keep = pltpu.make_async_copy(w_s, wall_hbm.at[t], w_sem.at[1])
+    keep.start()
+    n = 2
+    step = 64
+    rows = lambda k: pl.ds(pl.multiple_of(c * 128 + k * step, step), step)
+    own = {}
+    for i in range(n):
+        for slot, k, peer in ((0, i, right), (1, 1 - i, left)):
+            cp = pltpu.make_async_remote_copy(
+                src_ref=w_s.at[rows(k)], dst_ref=wall_hbm.at[t, rows(k)],
+                send_sem=ss.at[slot * n + k], recv_sem=rs.at[slot * n + k],
+                device_id={"tp": peer}, device_id_type=MESH)
+            cp.start()
+            own[slot, k] = cp
+    unpack_rows(msg_ref, x_s)
+
+    def hidden(j, carry):
+        pltpu.make_async_copy(g_s.at[j], g_s.at[j], g_sem.at[j]).wait()
+        pltpu.make_async_copy(u_s.at[j], u_s.at[j], u_sem.at[j]).wait()
+        gate = mm(x_s[...], g_s[j])
+        up = mm(x_s[...], u_s[j])
+        h_s[j] = (gate / (1.0 + jnp.exp(-gate)) * up).astype(BF)
+        return carry
+
+    lax.fori_loop(0, 4, hidden, 0)
+    passed = []
+    for slot, k, peer, who in ((0, 0, right, left), (1, 1, left, right)):
+        own[slot, k].wait_recv()
+        cp = pltpu.make_async_remote_copy(
+            src_ref=wall_hbm.at[who, rows(k)], dst_ref=wall_hbm.at[who, rows(k)],
+            send_sem=fs.at[k], recv_sem=fr.at[k],
+            device_id={"tp": peer}, device_id_type=MESH)
+        cp.start()
+        passed.append(cp)
+    back = order_mask(True)
+    for i in range(8):
+        out = []
+        for j in range(4):
+            if i == 0:
+                pltpu.make_async_copy(d_s.at[j], d_s.at[j], d_sem.at[j]).wait()
+            acc = None
+            for f in range(4):
+                part = mm(h_s[f, i * 64 : (i + 1) * 64, :], d_s[j, f * 256 : (f + 1) * 256, :])
+                acc = part if acc is None else acc + part
+            out.append(acc.astype(BF))
+        rows_out = jnp.concatenate(out, axis=0)
+        res_ref[i * 16 : (i + 1) * 16] = mm(back, rows_out).astype(BF).reshape(16, 16, 512)
+    own[0, 1].wait_recv()
+    own[1, 0].wait_recv()
+    shared = []
+    half = pl.ds(pl.multiple_of(c * 128, 128), 128)
+
+    def to_partner(i, who):
+        cp = pltpu.make_async_remote_copy(
+            src_ref=wall_hbm.at[who, half], dst_ref=wall_hbm.at[who, half],
+            send_sem=cs.at[i], recv_sem=cr.at[i],
+            device_id={"ep_2": 1 - c}, device_id_type=MESH)
+        cp.start()
+        shared.append(cp)
+
+    to_partner(0, left)
+    to_partner(1, right)
+    for cp in passed:
+        cp.wait()
+    to_partner(2, (t + 2) % 4)
+    for cp in own.values():
+        cp.wait_send()
+    keep.wait()
+    for cp in shared:
+        cp.wait()
+
+
+def combine_kernel(msg_ref, w_ref, shared_ref, res_ref, x_s):
+    unpack_rows(msg_ref, x_s)
+    for j in range(4):
+        cols = slice(j * 512, (j + 1) * 512)
+        both = mm(w_ref[...], x_s[:, cols])
+        res_ref[:, cols] = (both[:128] + both[128:] + shared_ref[:, cols]).astype(BF)
 
 
 def vspec(n):
     return [pl.BlockSpec(memory_space=VMEM)] * n
-
-
-def copy_for_each(value, axis):
-    copies = jnp.broadcast_to(value, (lax.axis_size(axis), *value.shape))
-    return lax.all_to_all(copies, axis, split_axis=0, concat_axis=0, tiled=True)
-
-
-def rms_rows(values, feature_gain):
-    wide_values = values.astype(F32)
-    inverse = lax.rsqrt(jnp.mean(wide_values * wide_values, axis=1, keepdims=True) + 1e-06)
-    return (wide_values * inverse * feature_gain).astype(BF)
 
 
 def per_device(
@@ -270,107 +484,105 @@
     routed_gate_weight, routed_up_weight, routed_down_weight,
     common_gate_weight, common_up_weight, common_down_weight,
 ):
-    normed_a = rms_rows(mixer_input_rows, mixer_norm_scale)
-    row_piece = copy_for_each(normed_a, "tp").reshape(512, -1)
-
-    normed_b = rms_rows(expert_input_rows, expert_norm_scale)
-    route_weight = 2.5 * router_weights / jnp.sum(router_weights, axis=1, keepdims=True)
-    token_count, top_count = routes.shape
-    expert_count = lax.axis_size(EP) * lax.axis_size("tp")
-    capacity = 2 * token_count * top_count // expert_count
-    slots = expert_count * capacity
-    chosen = routes.reshape(-1)
-    onehot = (chosen[:, None] == jnp.arange(expert_count, dtype=jnp.int32)[None, :]).astype(BF)
-    pairs = token_count * top_count
-    lower = (jnp.arange(pairs)[:, None] > jnp.arange(pairs)[None, :]).astype(BF)
-    counts = jnp.dot(lower, onehot, preferred_element_type=F32)
-    rank = jnp.sum(counts * onehot, axis=1).astype(jnp.int32)
-    slot_index = (chosen * capacity + rank).reshape(token_count, top_count)
-    slot_ids = jnp.arange(slots, dtype=jnp.int32)[None, :]
-    hit0 = slot_index[:, 0:1] == slot_ids
-    hit1 = slot_index[:, 1:2] == slot_ids
-    place = (hit0 | hit1).astype(BF)
-    outgoing = lax.dot_general(place, normed_b, (((0,), (0,)), ((), ())), preferred_element_type=F32)
-    outgoing = outgoing.astype(BF).reshape(expert_count, capacity, -1)
+    any_spec = pl.BlockSpec(memory_space=pl.ANY)
+    sds = jax.ShapeDtypeStruct
+    dma = pltpu.SemaphoreType.DMA
+    normed_a, normed_b, outgoing, weights = pl.pallas_call(
+        prep_kernel,
+        out_shape=(
+            sds((128, 2048), BF), sds((128, 2048), BF), sds((128, 16, 512), BF), sds((256, 512), BF),
+        ),
+        in_specs=vspec(6),
+        out_specs=tuple(vspec(4)),
+        cost_estimate=pl.CostEstimate(flops=1_000_000_000, bytes_accessed=5_000_000, transcendentals=0),
+        name="prep",
+    )(mixer_input_rows, mixer_norm_scale.reshape(1, -1), expert_input_rows,
+      expert_norm_scale.reshape(1, -1), routes, router_weights)
     arrived = lax.all_to_all(outgoing, EP_TP, split_axis=0, concat_axis=0, tiled=True)
-    flat_rows = arrived.reshape(slots, -1)
+
+    projected = pl.pallas_call(
+        ring_kernel,
+        out_shape=sds((512, 1280), F32),
+        in_specs=vspec(6),
+        out_specs=vspec(1)[0],
+        scratch_shapes=[VMEM((3, 128, 2048), BF), dma((8,)), dma((8,)), dma((4,)), dma((4,))],
+        compiler_params=pltpu.CompilerParams(collective_id=1, has_side_effects=True),
+        cost_estimate=pl.CostEstimate(flops=12_000_000_000, bytes_accessed=8_000_000, transcendentals=0),
+        name="ring_project",
+    )(normed_a, receive_weight, key_weight, value_weight, decay_weight, erase_weight)
+
+    result, w_all = pl.pallas_call(
+        expert_kernel,
+        out_shape=(sds((128, 16, 512), BF), sds((4, 256, 2048), BF)),
+        in_specs=vspec(1) + [any_spec] * 5,
+        out_specs=(vspec(1)[0], any_spec),
+        scratch_shapes=[
+            VMEM((512, 2048), BF),
+            VMEM((4, 2048, 256), BF), VMEM((4, 2048, 256), BF), VMEM((4, 1024, 512), BF),
+            VMEM((4, 512, 256), BF), VMEM((256, 2048), BF),
+            dma((4,)), dma((4,)), dma((4,)), dma((2,)),
+            dma((4,)), dma((4,)), dma((2,)), dma((2,)), dma((3,)), dma((3,)),
+        ],
+        compiler_params=pltpu.CompilerParams(collective_id=2, has_side_effects=True),
+        cost_estimate=pl.CostEstimate(flops=8_000_000_000, bytes_accessed=16_000_000, transcendentals=0),
+        name="experts",
+    )(arrived, routed_gate_weight[0], routed_up_weight[0], routed_down_weight[0], output_weight, projected)
+    returned = lax.all_to_all(result, EP_TP, split_axis=0, concat_axis=0, tiled=True)
 
     eb = jnp.repeat(erase_bias_table, 64).reshape(1, 256)
     out_l, rt, selft, tl = pl.pallas_call(
         mixer_kernel,
-        out_shape=(
-            jax.ShapeDtypeStruct((512, 256), F32),
-            jax.ShapeDtypeStruct((512, 256), BF),
-            jax.ShapeDtypeStruct((512, 256), F32),
-            jax.ShapeDtypeStruct((128, 256), BF),
-        ),
-        in_specs=vspec(9),
+        out_shape=(sds((512, 256), F32), sds((512, 256), BF), sds((512, 256), F32), sds((128, 256), BF)),
+        in_specs=vspec(4) + [any_spec],
         out_specs=tuple(vspec(4)),
-        scratch_shapes=[
-            VMEM((512, 1280), F32),
-            VMEM((512, 256), BF),
-            VMEM((1024, 256), BF),
-            VMEM((1024, 256), F32),
-            VMEM((64, 256), F32),
-        ],
-        cost_estimate=pl.CostEstimate(flops=6_000_000_000, bytes_accessed=10_000_000, transcendentals=0),
+        scratch_shapes=[VMEM((512, 256), BF), VMEM((1024, 256), BF), VMEM((1024, 256), F32), VMEM((64, 256), F32)],
+        cost_estimate=pl.CostEstimate(flops=6_000_000_000, bytes_accessed=6_000_000, transcendentals=0),
         name="mixer_local",
-    )(row_piece, receive_weight, key_weight, value_weight, decay_weight, erase_weight,
-      decay_bias_table, eb, self_token_scale.reshape(1, 256))
+    )(projected, decay_bias_table, eb, self_token_scale.reshape(1, 256), w_all)
 
     enter = pl.pallas_call(
         state_kernel,
-        out_shape=jax.ShapeDtypeStruct((64, 256), BF),
+        out_shape=sds((64, 256), BF),
         in_specs=vspec(1),
         out_specs=vspec(1)[0],
         scratch_shapes=[
-            VMEM((128, 256), BF),
-            VMEM((128, 256), BF),
-            VMEM((4, 128, 256), BF),
-            VMEM((128, 256), BF),
-            VMEM((4, 128, 256), BF),
-            pltpu.SemaphoreType.DMA, pltpu.SemaphoreType.DMA,
-            pltpu.SemaphoreType.DMA((4,)), pltpu.SemaphoreType.DMA((4,)),
-            pltpu.SemaphoreType.DMA((4,)), pltpu.SemaphoreType.DMA((4,)),
+            VMEM((128, 256), BF), VMEM((128, 256), BF), VMEM((4, 128, 256), BF),
+            VMEM((128, 256), BF), VMEM((4, 128, 256), BF),
+            dma, dma, dma((4,)), dma((4,)), dma((4,)), dma((4,)),
         ],
         compiler_params=pltpu.CompilerParams(collective_id=0, has_side_effects=True),
-        cost_estimate=pl.CostEstimate(flops=4_000_000_000, bytes_accessed=1_000_000, transcendentals=0),
+        cost_estimate=pl.CostEstimate(flops=6_000_000_000, bytes_accessed=1_000_000, transcendentals=0),
         name="state_exchange",
     )(tl)
 
-    partial = pl.pallas_call(
+    mixer_output = pl.pallas_call(
         finish_kernel,
-        out_shape=jax.ShapeDtypeStruct((512, 2048), BF),
-        in_specs=vspec(6),
+        out_shape=sds((128, 2048), BF),
+        in_specs=vspec(5) + [any_spec],
         out_specs=vspec(1)[0],
-        scratch_shapes=[VMEM((512, 256), BF)],
-        cost_estimate=pl.CostEstimate(flops=2_000_000_000, bytes_accessed=4_000_000, transcendentals=0),
+        scratch_shapes=[
+            VMEM((512, 256), BF), VMEM((4, 128, 256), BF), VMEM((4, 256, 2048), BF),
+            dma, dma((4,)), dma((4,)),
+        ],
+        compiler_params=pltpu.CompilerParams(collective_id=3, has_side_effects=True),
+        cost_estimate=pl.CostEstimate(flops=5_000_000_000, bytes_accessed=6_000_000, transcendentals=0),
         name="mixer_finish",
-    )(out_l, rt, selft, enter, head_norm_scale.reshape(1, 256), output_weight)
-    pieces = lax.all_to_all(partial.reshape(4, 128, 2048), "tp", split_axis=0, concat_axis=0, tiled=True)
-    mixer_output = pieces.astype(F32).sum(axis=0).astype(BF)
-
-    gate_part, up_part, down_part = routed_gate_weight[0], routed_up_weight[0], routed_down_weight[0]
-    expert_hidden = (
-        jax.nn.silu(jnp.dot(flat_rows, gate_part, preferred_element_type=F32))
-        * jnp.dot(flat_rows, up_part, preferred_element_type=F32)
-    ).astype(BF)
-    result = jnp.dot(expert_hidden, down_part, preferred_element_type=F32).astype(BF)
-    returned = lax.all_to_all(
-        result.reshape(expert_count, capacity, -1), EP_TP, split_axis=0, concat_axis=0, tiled=True
-    )
-    back_rows = returned.reshape(slots, -1)
-    weights = jnp.where(hit0, route_weight[:, 0:1], 0.0) + jnp.where(hit1, route_weight[:, 1:2], 0.0)
-    whi, wlo = split2(weights)
-    routed = jnp.dot(whi, back_rows, preferred_element_type=F32) + jnp.dot(
-        wlo, back_rows, preferred_element_type=F32
-    )
+    )(out_l, rt, selft, enter, head_norm_scale.reshape(1, 256), w_all)
+
     shared_hidden = (
         jax.nn.silu(jnp.dot(normed_b, common_gate_weight, preferred_element_type=F32))
         * jnp.dot(normed_b, common_up_weight, preferred_element_type=F32)
     ).astype(BF)
     shared_term = jnp.dot(shared_hidden, common_down_weight, preferred_element_type=F32)
-    mixed_b = (routed + shared_term).astype(BF)
+    mixed_b = pl.pallas_call(
+        combine_kernel,
+        out_shape=sds((128, 2048), BF),
+        in_specs=vspec(3),
+        out_specs=vspec(1)[0],
+        scratch_shapes=[VMEM((512, 2048), BF)],
+        cost_estimate=pl.CostEstimate(flops=1_000_000_000, bytes_accessed=4_000_000, transcendentals=0),
+        name="combine",
+    )(returned, weights, shared_term)
     return (mixer_output, mixed_b)
 
 

time: 161 us -> 158 us (0.981)
  Pallas kernels: 40.2 us -> 122 us
  waiting for transfers between devices: 47.5 us -> 0.01 us
  matrix products: 24 us -> 4.85 us
  local copies, waits for them, and re-layouts: 16 us -> 9.68 us
  other arithmetic: 5.73 us -> 0 us
  starting transfers between devices: 25.9 us -> 20.3 us
    pallas_call x3 -> x7, Pallas kernels: 40.2 us -> 122 us  [the longest x1 42.4 us: per_device(): pl.pallas_call(ring_kernel, out_shape=sds((512, 1280), F32), in_specs=vsp...]
    all_to_all x3 -> x1, waiting for transfers between devices: 47.5 us -> 0.01 us  [per_device(): lax.all_to_all(result, EP_TP, split_axis=0, concat_axis=0, tiled=True)]
    dot_general x6 -> x0, matrix products: 20.6 us -> none  [the longest x1 9.97 us: per_device(): jnp.dot(expert_hidden, down_part, preferred_element_type=F32).astype(BF)]
    reshape x4 -> x0, local copies, waits for them, and re-layouts: 11 us -> none  [the longest x1 4.11 us: per_device(): result.reshape(expert_count, capacity, -1)]
    all_to_all x3 -> x1, starting transfers between devices: 15.9 us -> 8.79 us  [per_device(): lax.all_to_all(result, EP_TP, split_axis=0, concat_axis=0, tiled=True)]
    unnamed x26 -> x16, local copies, waits for them, and re-layouts: 1.74 us -> 8.3 us
    reduce_sum x4 -> x0, other arithmetic: 4.46 us -> none  [the longest x1 2.92 us: per_device(): mixer_output = pieces.astype(F32).sum(axis=0).astype(BF)]
  transfers between devices with their start and end apart: 4 -> 2, of which waited for: 3 -> 0; matrix products, arithmetic and copies ran while one was open for 23% -> 5% of each run, Pallas kernels for 25% -> 54%
where the time goes in v2:
time: 158 us; the launch traced here: 157 us
  Pallas kernels  122 us (77%)
  starting transfers between devices  20.3 us (13%)
  local copies, waits for them, and re-layouts  9.68 us (6%)
  matrix products  4.85 us (3%)
    pallas_call x1, Pallas kernels, per_device(): pl.pallas_call(ring_kernel, out_shape=sds((512, 1280), F32), in_specs=vsp...  42.4 us
    pallas_call x1, Pallas kernels, per_device(): pl.pallas_call(expert_kernel, out_shape=(sds((128, 16, 512), BF), sds((4,...  28.9 us
    pallas_call x1, Pallas kernels, per_device(): pl.pallas_call(state_kernel, out_shape=sds((64, 256), BF), in_specs=vspec...  21.5 us
    all_to_all x1, starting transfers between devices, per_device(): lax.all_to_all(outgoing, EP_TP, split_axis=0, concat_axis=0, tiled=True)  11.5 us
    pallas_call x1, Pallas kernels, per_device(): pl.pallas_call(mixer_kernel, out_shape=(sds((512, 256), F32), sds((512, 2...  11.5 us
    all_to_all x1, starting transfers between devices, per_device(): lax.all_to_all(result, EP_TP, split_axis=0, concat_axis=0, tiled=True)  8.79 us
    pallas_call x1, Pallas kernels, per_device(): pl.pallas_call(finish_kernel, out_shape=sds((128, 2048), BF), in_specs=vs...  8.75 us
    unnamed x16, local copies, waits for them, and re-layouts  8.3 us
  transfers between devices with their start and end apart: 2, of which 0 were waited for; matrix products, arithmetic and copies ran while one was open for 5% of the time, Pallas kernels for 54%

profile of v2, /device:TPU:1, one launch (start us, length us, event | category | flops | bytes accessed | tf_op | source)
XLA Modules:
  0.0 157.1 jit_solution(17010277582928902670)
XLA Ops:
  0.6 0.0 copy-start
  0.6 1.5 copy.24.routes_ref
  2.1 1.4 copy.25.rw_ref
  3.5 4.5 %prep.1 = (bf16[128,2048]{1,0:T(8,128)(2,1)}, bf16[128,2048]{1,0:T(8,128)(2,1)}, bf16[128,16,512]{2,1,0:T(8,128)(2,1)}, bf16[256,512]{1,0:T(8,128)(2,1)}) custom-call(bf16[128,2048]{1,0:T(8,128)(2,1)} %a_ref.1, f32[1,2048]{1,0:T(1,128)} %bitcast.14, bf16[128,2048]{1,0:T(8,128)(2,1)} %b_ref.1, f32[1,2048]{1,0:T(1,128)} %bitcast.15, ...), custom_call_target="tpu_custom_call" | custom-call | flops 1000000000 | bytes 5000000 | tf_op jit(solution)/shard_map/prep/pallas_call | solution.py:490
  8.0 0.0 copy-start.3
  8.0 0.0 copy-start.5
  8.0 0.0 copy-start.4
  8.0 11.5 %all-to-all-start = ((bf16[128,16,512]{2,1,0:T(8,128)(2,1)}), bf16[128,16,512]{2,1,0:T(8,128)(2,1)S(1)}, u32[]{:S(2)}, u32[]{:S(2)}) async-start(bf16[128,16,512]{2,1,0:T(8,128)(2,1)} %get-tuple-element.13), calls=%async_computation | async-start | bytes 4194304 | tf_op jit(solution)/shard_map/all_to_all | solution.py:501
  19.5 0.0 copy-done.3
  19.5 0.9 copy.26.db_ref
  20.4 0.0 copy-done.5
  20.4 0.1 broadcast_in_dim.3
  20.5 0.7 reshape_reshape.3.eb_ref
  21.1 0.0 copy-done.4
  21.1 0.7 reshape.18.st_ref
  21.8 42.4 %ring_project.1.after_ref.pr_ref = f32[512,1280]{1,0:T(8,128)} custom-call(bf16[128,2048]{1,0:T(8,128)(2,1)} %get-tuple-element.12.x_ref, bf16[2048,256]{1,0:T(8,128)(2,1)} %wr_ref.1, bf16[2048,256]{1,0:T(8,128)(2,1)} %wk_ref.1, bf16[2048,256]{1,0:T(8,128)(2,1)} %wv_ref.1, bf16[2048,256]{1,0:T(8,128)(2,1)} %wd_ref.1, bf16[2048,256]{1,0:T(8,128)(2,1)} %we_ref.1), custom_call_target="tpu_custom_call" | custom-call | flops 12000000000 | bytes 8000000 | tf_op jit(solution)/shard_map/ring_project/pallas_call | solution.py:503
  64.2 0.0 all-to-all-done.msg_ref
  64.2 0.0 copy-start.2
  64.2 1.3 copy-done.2
  65.5 28.9 %experts.1 = (bf16[128,16,512]{2,1,0:T(8,128)(2,1)}, bf16[4,256,2048]{2,1,0:T(8,128)(2,1)}) custom-call(bf16[128,16,512]{2,1,0:T(8,128)(2,1)} %copy-done.2, bf16[2048,1024]{1,0:T(8,128)(2,1)} %bitcast.11, bf16[2048,1024]{1,0:T(8,128)(2,1)} %bitcast.12, bf16[1024,2048]{1,0:T(8,128)(2,1)} %bitcast.13, bf16[256,2048]{1,0:T(8,128)(2,1)} %w_hbm.1, ...), custom_call_target="tpu_custom_call" | custom-call | flops 8000000000 | bytes 16000000 | tf_op jit(solution)/shard_map/experts/pallas_call | solution.py:514
  94.5 8.8 %all-to-all-start.1 = ((bf16[128,16,512]{2,1,0:T(8,128)(2,1)}), bf16[128,16,512]{2,1,0:T(8,128)(2,1)S(1)}, u32[]{:S(2)}, u32[]{:S(2)}) async-start(bf16[128,16,512]{2,1,0:T(8,128)(2,1)} %get-tuple-element.19), calls=%async_computation.1 | async-start | bytes 4194304 | tf_op jit(solution)/shard_map/all_to_all | solution.py:530
  103.3 1.7 %fusion.9 = f32[128,256]{1,0:T(8,128)S(1)} fusion(bf16[128,2048]{1,0:T(8,128)(2,1)} %get-tuple-element.21, bf16[2048,256]{1,0:T(8,128)(2,1)} %param.41), kind=kOutput, calls=%fused_computation.10 | convolution fusion | flops 134217728 | bytes 1703936 | tf_op jit(solution)/shard_map/dot_general | solution.py:573
  105.0 0.0 copy-done
  105.0 3.2 %fusion.1.shared_ref = f32[128,2048]{1,0:T(8,128)} fusion(bf16[256,2048]{1,0:T(8,128)(2,1)S(1)} %copy-done, bf16[128,2048]{1,0:T(8,128)(2,1)} %get-tuple-element.21, bf16[2048,256]{1,0:T(8,128)(2,1)} %param.42, f32[128,256]{1,0:T(8,128)S(1)} %fusion.9), kind=kOutput, calls=%fused_computation.2 | convolution fusion | flops 268632064 | bytes 3801088 | tf_op jit(solution)/shard_map/dot_general | solution.py:576
  108.1 11.5 %mixer_local.1 = (f32[512,256]{1,0:T(8,128)}, bf16[512,256]{1,0:T(8,128)(2,1)}, f32[512,256]{1,0:T(8,128)}, bf16[128,256]{1,0:T(8,128)(2,1)}) custom-call(f32[512,1280]{1,0:T(8,128)} %ring_project.1.after_ref.pr_ref, f32[512,4]{1,0:T(8,128)} %copy.26.db_ref, f32[1,256]{1,0:T(1,128)} %reshape_reshape.3.eb_ref, f32[1,256]{1,0:T(1,128)} %reshape.18.st_ref, ...), custom_call_target="tpu_custom_call" | custom-call | flops 6000000000 | bytes 6000000 | tf_op jit(solution)/shard_map/mixer_local/pallas_call | solution.py:533
  119.6 21.5 %state_exchange.1.enter_ref = bf16[64,256]{1,0:T(8,128)(2,1)} custom-call(bf16[128,256]{1,0:T(8,128)(2,1)} %get-tuple-element.18.tl_ref), custom_call_target="tpu_custom_call" | custom-call | flops 6000000000 | bytes 1000000 | tf_op jit(solution)/shard_map/state_exchange/pallas_call | solution.py:543
  141.1 8.7 %mixer_finish.1 = bf16[128,2048]{1,0:T(8,128)(2,1)} custom-call(f32[512,256]{1,0:T(8,128)} %get-tuple-element.15.out_ref, bf16[512,256]{1,0:T(8,128)(2,1)} %get-tuple-element.16.rt_ref, f32[512,256]{1,0:T(8,128)} %get-tuple-element.17.self_ref, bf16[64,256]{1,0:T(8,128)(2,1)} %state_exchange.1.enter_ref, f32[1,256]{1,0:T(1,128)} %bitcast.16, ...), custom_call_target="tpu_custom_call" | custom-call | flops 5000000000 | bytes 6000000 | tf_op jit(solution)/shard_map/mixer_finish/pallas_call | solution.py:558
  149.9 0.0 all-to-all-done.1.msg_ref
  149.9 0.0 copy-start.1
  149.9 1.3 copy-done.1
  151.2 4.0 %combine.1 = bf16[128,2048]{1,0:T(8,128)(2,1)} custom-call(bf16[128,16,512]{2,1,0:T(8,128)(2,1)} %copy-done.1, bf16[256,512]{1,0:T(8,128)(2,1)} %get-tuple-element.20.w_ref, f32[128,2048]{1,0:T(8,128)} %fusion.1.shared_ref), custom_call_target="tpu_custom_call" | custom-call | flops 1000000000 | bytes 4000000 | tf_op jit(solution)/shard_map/combine/pallas_call | solution.py:577
  155.2 1.9 %copy.28 = bf16[128,2048]{1,0:T(8,128)(2,1)} copy(bf16[128,2048]{1,0:T(8,128)(2,1)} %mixer_finish.1) | data formatting | bytes 1048576
Async XLA Ops:
  0.6 104.4 %copy-start = (bf16[256,2048]{1,0:T(8,128)(2,1)S(1)}, bf16[256,2048]{1,0:T(8,128)(2,1)}, u32[]{:S(2)}) copy-start(bf16[256,2048]{1,0:T(8,128)(2,1)} %param.43) | copy-start | bytes 3145732
  8.0 11.5 %copy-start.3 = (f32[512,4]{0,1:T(4,128)S(1)}, f32[512,4]{0,1:T(4,128)}, u32[]{:S(2)}) copy-start(f32[512,4]{0,1:T(4,128)} %param.24) | copy-start | bytes 24580
  8.0 12.4 %copy-start.5 = (f32[4]{0:T(128)S(1)}, f32[4]{0:T(128)}, u32[]{:S(2)}) copy-start(f32[4]{0:T(128)} %param.25) | copy-start | bytes 52
  8.0 13.1 %copy-start.4 = (f32[4,64]{1,0:T(4,128)S(1)}, f32[4,64]{1,0:T(4,128)}, u32[]{:S(2)}) copy-start(f32[4,64]{1,0:T(4,128)} %param.31) | copy-start | bytes 3076
  8.0 56.2 %all-to-all-start = ((bf16[128,16,512]{2,1,0:T(8,128)(2,1)}), bf16[128,16,512]{2,1,0:T(8,128)(2,1)S(1)}, u32[]{:S(2)}, u32[]{:S(2)}) async-start(bf16[128,16,512]{2,1,0:T(8,128)(2,1)} %get-tuple-element.13), calls=%async_computation | async-start | bytes 4194304 | tf_op jit(solution)/shard_map/all_to_all | solution.py:501
  64.2 1.3 copy-start.2
  94.5 55.4 %all-to-all-start.1 = ((bf16[128,16,512]{2,1,0:T(8,128)(2,1)}), bf16[128,16,512]{2,1,0:T(8,128)(2,1)S(1)}, u32[]{:S(2)}, u32[]{:S(2)}) async-start(bf16[128,16,512]{2,1,0:T(8,128)(2,1)} %get-tuple-element.19), calls=%async_computation.1 | async-start | bytes 4194304 | tf_op jit(solution)/shard_map/all_to_all | solution.py:530
  149.9 1.3 copy-start.1

commit v3 on v2

v3 whole, which is shorter than its diff:
```python
import functools

import jax
import jax.numpy as jnp
from jax import lax
from jax.experimental import pallas as pl
from jax.experimental.pallas import tpu as pltpu
from jax.sharding import Mesh
from jax.sharding import PartitionSpec as P

EP = ("ep_0", "ep_1", "ep_2")
EP_TP = ("ep_0", "ep_1", "ep_2", "tp")
MESH = pl.DeviceIdType.MESH
BF = jnp.bfloat16
F32 = jnp.float32
VMEM = pltpu.VMEM
CHUNK = 64
PAIR = 128


def mm(a, b):
    return lax.dot_general(a, b, (((1,), (0,)), ((), ())), preferred_element_type=F32)


def mm_t(a, b):
    return lax.dot_general(a, b, (((1,), (1,)), ((), ())), preferred_element_type=F32)


def mm_tn(a, b):
    return lax.dot_general(a, b, (((0,), (0,)), ((), ())), preferred_element_type=F32)


def split2(x):
    hi = x.astype(BF)
    lo = (x - hi.astype(F32)).astype(BF)
    return hi, lo


def iota(shape, dim):
    return lax.broadcasted_iota(jnp.int32, shape, dim)


def pair_mask():
    return (iota((PAIR, PAIR), 0) // 64) == (iota((PAIR, PAIR), 1) // 64)


def block_diag(x, mask):
    return jnp.concatenate([x, x], axis=0) * mask


def head_sums(x, mask):
    hi, lo = split2(x)
    return mm(hi, mask) + mm(lo, mask)


def split3(x):
    hi = x.astype(BF)
    rest = x - hi.astype(F32)
    mid = rest.astype(BF)
    return jnp.concatenate([hi, mid, (rest - mid.astype(F32)).astype(BF)], axis=0)


def mixer_body(pr_ref, db_ref, eb_ref, st_ref, out_ref, rt_ref, self_ref, tl_ref, r_s, e_s, l_s, d_s, db_s):
    n_rows = pr_ref.shape[1]
    n_chunks = n_rows // CHUNK
    group = 4
    mask_b = pair_mask()
    mask = mask_b.astype(F32).astype(BF)

    t_i = iota((CHUNK, PAIR), 0)
    s_i = iota((CHUNK, PAIR), 1) % 64
    strict = t_i > s_i
    causal = t_i >= s_i
    eye = (t_i == s_i).astype(F32)
    lane_lo = iota((CHUNK, PAIR), 1) < 64
    heads_of = (iota((12, 256), 0) % 4 == iota((12, 256), 1) // 64).astype(F32).astype(BF)
    db_s[...] = mm_tn(split3(db_ref[...]), heads_of)
    twice = jnp.concatenate([st_ref[...], st_ref[...]], axis=1)
    st = [jnp.where(lane_lo[0:1], twice[2 * p : 2 * p + 1], twice[2 * p + 1 : 2 * p + 2]) for p in range(2)]
    eb = [jnp.where(lane_lo[0:1], eb_ref[0:1, 2 * p : 2 * p + 1], eb_ref[0:1, 2 * p + 1 : 2 * p + 2]) for p in range(2)]
    tril = (iota((CHUNK, CHUNK), 0) >= iota((CHUNK, CHUNK), 1)).astype(F32).astype(BF)

    def do_group(g, carry):
        units = []
        for cc in range(group):
            for p in range(2):
                r0 = pl.multiple_of((g * group + cc) * CHUNK, CHUNK)
                rows = pl.ds(r0, CHUNK)
                lanes = slice(p * PAIR, (p + 1) * PAIR)
                col = lambda j: pr_ref[j, rows, lanes]
                r, k, v, dp, ep = (col(j) for j in range(5))
                ld = -0.6065306597126334 / (1.0 + jnp.exp(-(dp + db_s[rows, lanes])))
                er = 1.0 / (1.0 + jnp.exp(-(ep + eb[p])))
                u = k * lax.rsqrt(head_sums(k * k, mask) + 1e-06)
                self_ref[rows, lanes] = head_sums(r * k * st[p], mask) * v
                hi, lo = split2(ld)
                cum = mm(tril, hi) + mm(tril, lo)
                end = cum[CHUNK - 1 : CHUNK, :]
                eci = jnp.exp(-cum)
                a = (-u * jnp.exp(cum - ld)).astype(BF)
                ri = r * jnp.exp(cum)
                ue = u * er
                b = (ue * eci).astype(BF)
                ko = (k * eci).astype(BF)
                tail = jnp.exp(end - cum)
                bt = (ue * tail).astype(BF)
                kt = (k * tail).astype(BF)
                ar = jnp.concatenate([a, ri.astype(BF)], axis=0)
                m13 = mm_t(ar, block_diag(b, mask))
                m24 = mm_t(ar, block_diag(ko, mask))
                m1 = jnp.where(strict, m13[:CHUNK], 0.0)
                m3 = jnp.where(causal, m13[CHUNK:], 0.0).astype(BF)
                m24 = jnp.concatenate(
                    [jnp.where(strict, m24[:CHUNK], 0.0), jnp.where(causal, m24[CHUNK:], 0.0)], axis=0
                ).astype(BF)
                vb = v.astype(BF)
                mv = mm(m24, block_diag(vb, mask))
                x = eye + jnp.where((t_i // 2) == (s_i // 2), m1, 0.0)
                units.append(
                    dict(rows=rows, lanes=lanes, p=p, r0=r0, a=a, ri=ri, m1=m1, m3=m3, mv=mv, x=x,
                         bt=bt, kt=kt, vb=vb, end=end)
                )
        size = 2
        while size < CHUNK:
            corner = ((t_i // (2 * size)) == (s_i // (2 * size))) & ((t_i // size) != (s_i // size))
            for n in units:
                xb = n["x"].astype(BF)
                n["xb"] = xb
                c = jnp.where(corner, n["m1"], 0.0).astype(BF)
                n["y"] = mm(xb, block_diag(c, mask)).astype(BF)
            for n in units:
                n["x"] = n["x"] + mm(n["y"], block_diag(n["xb"], mask))
            size *= 2
        for n in units:
            right = jnp.concatenate(
                [block_diag(n["a"], mask), block_diag(n["mv"][:CHUNK].astype(BF), mask)], axis=1
            )
            n["pq"] = mm(n["x"].astype(BF), right).astype(BF)
        for n in units:
            pb, qb = n["pq"][:, :PAIR], n["pq"][:, PAIR:]
            m3pq = mm(n["m3"], jnp.concatenate([block_diag(pb, mask), block_diag(qb, mask)], axis=1))
            r_s[n["rows"], n["lanes"]] = (n["ri"] + m3pq[:, :PAIR]).astype(BF)
            out_ref[n["rows"], n["lanes"]] = m3pq[:, PAIR:] + n["mv"][CHUNK:]
            big = pl.ds(pl.multiple_of(n["r0"] * 2, PAIR), PAIR)
            e_s[big, n["lanes"]] = (mm_tn(pb, n["bt"]) * mask).astype(BF)
            left = jnp.concatenate([qb, n["vb"]], axis=0)
            right = jnp.concatenate([n["bt"], n["kt"]], axis=0)
            l_s[big, n["lanes"]] = mm_tn(left, right) * mask
            small = pl.ds(pl.multiple_of(n["r0"] // 8, 8), 8)
            d_s[small, n["lanes"]] = jnp.broadcast_to(jnp.exp(n["end"]), (8, PAIR))
        return carry

    lax.fori_loop(0, n_chunks // group, do_group, 0)

    eye2 = (iota((PAIR, PAIR), 0) == iota((PAIR, PAIR), 1)).astype(F32)
    state = [jnp.concatenate([jnp.zeros((PAIR, PAIR), F32), eye2], axis=0) for _ in range(2)]
    for c in range(n_chunks):
        rows = slice(c * CHUNK, (c + 1) * CHUNK)
        big = slice(c * PAIR, (c + 1) * PAIR)
        for p in range(2):
            lanes = slice(p * PAIR, (p + 1) * PAIR)
            sb = state[p].astype(BF)
            o = mm_t(r_s[rows, lanes], sb)
            out_ref[rows, lanes] = out_ref[rows, lanes] + o[:, :PAIR]
            rt_ref[rows, lanes] = o[:, PAIR:].astype(BF)
            decayed = state[p] * d_s[c * 8 : c * 8 + 1, lanes]
            moved = mm(sb, e_s[big, lanes])
            state[p] = decayed + moved
            state[p] = jnp.concatenate([state[p][:PAIR] + l_s[big, lanes], state[p][PAIR:]], axis=0)
    for p in range(2):
        lanes = slice(p * PAIR, (p + 1) * PAIR)
        tl_ref[0:64, lanes] = (state[p][PAIR : PAIR + 64] + state[p][PAIR + 64 :]).astype(BF)
        tl_ref[64:128, lanes] = (state[p][0:64] + state[p][64:128]).astype(BF)


def mixer_kernel(
    pr_ref, db_ref, eb_ref, st_ref, s0_hbm, s1_hbm,
    out_ref, rt_ref, self_ref, enter_ref, t0_hbm, t1_hbm,
    r_s, e_s, l_s, d_s, db_s, tl, hop, xs, xr, lsem, *state_scratch,
):
    z, y, c = lax.axis_index("ep_0"), lax.axis_index("ep_1"), lax.axis_index("ep_2")
    t = lax.axis_index("tp")
    takes = [pltpu.make_async_copy(s_hbm.at[:, :, c * 4 + t], hop.at[i], lsem.at[i])
             for i, s_hbm in enumerate((s0_hbm, s1_hbm))]
    for cp in takes:
        cp.start()
    signal_all(
        [{"ep_2": (c + dc) % 2, "tp": (t + dt) % 4} for dc in range(2) for dt in range(4) if dc or dt]
        + [{"ep_1": (y + d) % 4} for d in range(1, 4)]
        + [{"ep_0": (z + d) % 4} for d in range(1, 4)]
    )
    moves = []
    for dt in (1, 3, 2, 0):
        for dc in range(2):
            if not (dt or dc):
                continue
            pc, pt = (c + dc) % 2, (t + dt) % 4
            for i, (s_hbm, t_hbm) in enumerate(((s0_hbm, t0_hbm), (s1_hbm, t1_hbm))):
                at = i * 8 + dc * 4 + dt
                moves.append(
                    send(s_hbm.at[:, :, pc * 4 + pt], t_hbm.at[c * 4 + t], xs.at[at], xr.at[at],
                         {"ep_2": pc, "tp": pt}))
    for cp in takes:
        cp.wait()
    puts = [pltpu.make_async_copy(hop.at[i], t_hbm.at[c * 4 + t], lsem.at[i])
            for i, t_hbm in enumerate((t0_hbm, t1_hbm))]
    for cp in puts:
        cp.start()
    mixer_body(pr_ref, db_ref, eb_ref, st_ref, out_ref, rt_ref, self_ref, tl, r_s, e_s, l_s, d_s, db_s)
    state_body(tl, enter_ref, *state_scratch)
    for cp in puts + moves:
        cp.wait()


def state_body(tl_ref, enter_ref, cbuf, ysend, ybuf, zsend, zbuf, cs, cr, ys, yr, zs, zr):
    z, y, c = lax.axis_index("ep_0"), lax.axis_index("ep_1"), lax.axis_index("ep_2")
    mask = pair_mask().astype(F32).astype(BF)

    def times(left, t):
        return jnp.concatenate(
            [mm(left[:, q * PAIR : (q + 1) * PAIR].astype(BF),
                block_diag(t[:, q * PAIR : (q + 1) * PAIR].astype(BF), mask)) for q in range(2)],
            axis=1,
        )

    def compose(early, late):
        joined = times(early, late[:64])
        return jnp.concatenate([joined[:64], joined[64:] + late[64:]], axis=0)

    cp = pltpu.make_async_remote_copy(
        src_ref=tl_ref, dst_ref=cbuf, send_sem=cs, recv_sem=cr,
        device_id={"ep_2": 1 - c}, device_id_type=MESH)
    cp.start()
    cp.wait()
    mine = tl_ref[...].astype(F32)
    other = cbuf[...].astype(F32)
    first = jnp.where(c == 0, mine, other)
    second = jnp.where(c == 0, other, mine)

    def exchange(value, send, buf, ss, rs, axis, me):
        send[...] = value.astype(BF)
        copies = []
        for d in range(1, 4):
            cp = pltpu.make_async_remote_copy(
                src_ref=send, dst_ref=buf.at[d], send_sem=ss.at[d], recv_sem=rs.at[d],
                device_id={axis: (me + d) % 4}, device_id_type=MESH)
            cp.start()
            copies.append(cp)
        buf[0] = value.astype(BF)
        for cp in copies:
            cp.wait()

    exchange(compose(first, second), ysend, ybuf, ys, yr, "ep_1", y)
    run = ybuf[y % 4].astype(F32)
    ident = (iota((64, 256), 0) == iota((64, 256), 1) % 64).astype(F32)
    before = jnp.concatenate([ident, jnp.zeros((64, 256), F32)], axis=0)
    for j in range(1, 4):
        before = jnp.where(y == j, run, before)
        run = compose(run, ybuf[(y - j + 4) % 4].astype(F32))
    exchange(run, zsend, zbuf, zs, zr, "ep_0", z)
    state = jnp.zeros((64, 256), F32)
    enter = state
    for j in range(0, 3):
        piece = zbuf[(z - j + 4) % 4].astype(F32)
        state = (times(state, piece[:64]) if j else 0.0) + piece[64:]
        enter = jnp.where(z == j + 1, state, enter)
    enter = times(enter, before[:64]) + before[64:]
    enter = jnp.where(c == 0, enter, times(enter, first[:64]) + first[64:])
    enter_ref[...] = enter.astype(BF)


def finish_kernel(
    out_ref, rt_ref, self_ref, enter_ref, gain_ref, w_hbm, near_hbm, far_hbm, other_hbm, res_ref,
    heads, landed, w_s, w_sem, ss, rs,
):
    t, c = lax.axis_index("tp"), lax.axis_index("ep_2")
    mine = pl.ds(pl.multiple_of(c * 128, 128), 128)
    theirs = pl.ds(pl.multiple_of((1 - c) * 128, 128), 128)
    loads = [pltpu.make_async_copy(w_hbm, w_s.at[t], w_sem.at[0])]
    for i, src in enumerate((near_hbm.at[0], near_hbm.at[1], far_hbm)):
        who = (t + (3, 1, 2)[i]) % 4
        loads.append(pltpu.make_async_copy(src, w_s.at[who, mine], w_sem.at[1 + i]))
        loads.append(pltpu.make_async_copy(other_hbm.at[i], w_s.at[who, theirs], w_sem.at[4 + i]))
    for cp in loads:
        cp.start()
    barrier = pltpu.get_barrier_semaphore()
    for d in range(1, 4):
        pl.semaphore_signal(barrier, inc=1, device_id={"tp": (t + d) % 4}, device_id_type=MESH)
    mask = pair_mask().astype(F32).astype(BF)
    for p in range(2):
        lanes = slice(p * PAIR, (p + 1) * PAIR)
        ent = block_diag(enter_ref[:, lanes], mask)
        o = out_ref[:, lanes] + mm_t(rt_ref[:, lanes], ent)
        o = o - head_sums(o, mask) * (1.0 / 64)
        var = head_sums(o * o, mask) * (1.0 / 64)
        h = o * lax.rsqrt(var + 0.00064) * gain_ref[:, lanes] + self_ref[:, lanes]
        heads[:, lanes] = h.astype(BF)
    pl.semaphore_wait(barrier, 3)
    copies = []
    for d in (2, 1, 3):
        peer = (t + d) % 4
        copies.append(
            send(heads.at[pl.ds(pl.multiple_of(peer * 128, 128), 128)], landed.at[d], ss.at[d], rs.at[d],
                 {"tp": peer}))
    for cp in loads:
        cp.wait()
    own = heads[pl.ds(pl.multiple_of(t * 128, 128), 128), :]
    for cp in copies:
        cp.wait()
    for j in range(4):
        cols = slice(j * 512, (j + 1) * 512)
        total = mm(own, w_s[t, :, cols])
        for d in range(1, 4):
            total = total + mm(landed[d], w_s[(t + 4 - d) % 4, :, cols])
        res_ref[:, cols] = total.astype(BF)


def prep_kernel(a_ref, ga_ref, b_ref, gb_ref, routes_ref, rw_ref, na_ref, nb_ref, m0_ref, m1_ref, w_ref):
    for x_ref, g_ref, o_ref in ((a_ref, ga_ref, na_ref), (b_ref, gb_ref, nb_ref)):
        x = x_ref[...].astype(F32)
        inverse = lax.rsqrt(jnp.mean(x * x, axis=1, keepdims=True) + 1e-06)
        o_ref[...] = (x * inverse * g_ref[...]).astype(BF)
    n = 128
    chosen = routes_ref[...].astype(F32)
    c0, c1 = chosen[0:1, :], chosen[1:2, :]
    sub = iota((n, n), 0)
    sub_f = sub.astype(F32)
    oh0 = jnp.where(c0 == sub_f, 1.0, 0.0)
    oh1 = jnp.where(c1 == sub_f, 1.0, 0.0)
    before = (sub < iota((n, n), 1)).astype(F32).astype(BF)
    counts = mm((oh0 + oh1).astype(BF), before)
    s0 = c0 * 4.0 + jnp.sum(counts * oh0, axis=0, keepdims=True)
    s1 = c1 * 4.0 + jnp.sum(counts * oh1, axis=0, keepdims=True)
    rw = rw_ref[...]
    rw = 2.5 * rw / (rw[0:1, :] + rw[1:2, :])
    slot = iota((512, n), 0).astype(F32)
    w = jnp.where(s0 == slot, rw[0:1, :], 0.0) + jnp.where(s1 == slot, rw[1:2, :], 0.0)
    hi, lo = split2(w)
    w_ref[:, 0:n] = hi
    w_ref[:, n:] = lo
    nb = nb_ref[...]
    pieces = jnp.concatenate([nb[:, q * 512 : (q + 1) * 512] for q in range(4)], axis=0)
    row = iota((256, n), 0)
    for i in range(8):
        ident = ((i * 16 + row // 16) * 4 + row % 4).astype(F32)
        hit = jnp.where((s0 == ident) | (s1 == ident), 1.0, 0.0)
        piece = (row // 4) % 4
        oh = jnp.concatenate([jnp.where(piece == q, hit, 0.0).astype(BF) for q in range(4)], axis=1)
        res = mm(oh, pieces).astype(BF)
        for h in range(2):
            z, y = i // 2, (i % 2) * 2 + h
            half = res[h * 128 : (h + 1) * 128]
            m0_ref[y, z] = half[:, :256].reshape(8, 16, 256)
            m1_ref[z, y] = half[:, 256:].reshape(8, 16, 256)


def order_mask(back):
    r, l = iota((256, 256), 0), iota((256, 256), 1)
    if back:
        r, l = l, r
    want = ((l // 4) % 4 == r // 64) & (l // 16 == (r % 64) // 4) & (l % 4 == r % 4)
    return want.astype(F32).astype(BF)


def unpack_block(order, block, x_ref, i):
    rows = mm(order, block).astype(BF)
    for q in range(4):
        x_ref[i * 64 : (i + 1) * 64, q * 512 : (q + 1) * 512] = rows[q * 64 : (q + 1) * 64]


def signal_all(peers):
    barrier = pltpu.get_barrier_semaphore()
    for peer in peers:
        pl.semaphore_signal(barrier, inc=1, device_id=peer, device_id_type=MESH)
    pl.semaphore_wait(barrier, len(peers))


def send(src, dst, ss, rs, peer):
    cp = pltpu.make_async_remote_copy(
        src_ref=src, dst_ref=dst, send_sem=ss, recv_sem=rs, device_id=peer, device_id_type=MESH)
    cp.start()
    return cp


def ring_kernel(
    x_ref, m0_ref, m1_ref, wr, wk, wv, wd, we, wo,
    pr_ref, s0_ref, s1_ref, near_ref,
    held, r0, r1, w_s, wsem, ss, rs, fs, fr, as_, ar, bs, br, os_, or_, lsem,
):
    z, y, t = lax.axis_index("ep_0"), lax.axis_index("ep_1"), lax.axis_index("tp")
    c = lax.axis_index("ep_2")
    right, left = (t + 1) % 4, (t + 3) % 4
    loads = []
    for j, w in enumerate((wr, wk, wv, wd, we)):
        cp = pltpu.make_async_copy(w, w_s.at[j], wsem.at[j])
        cp.start()
        loads.append(cp)
    signal_all(
        [{"tp": right}, {"tp": left}]
        + [{"ep_1": (y + d) % 4} for d in range(1, 4)]
        + [{"ep_0": (z + d) % 4} for d in range(1, 4)]
    )
    n = 4
    step = 128 // n
    rows = lambda k: pl.ds(k * step, step)
    own = {}
    first = []
    for i in range(n):
        for slot, k, peer in ((0, i, right), (1, (i + n // 2) % n, left)):
            own[slot, k] = send(
                x_ref.at[rows(k)], held.at[slot, rows(k)], ss.at[slot * n + k], rs.at[slot * n + k], {"tp": peer})
        if i == 0:
            for d in (1, 3, 2):
                first.append(send(m0_ref.at[(y + d) % 4], r0.at[y], as_.at[d], ar.at[d], {"ep_1": (y + d) % 4}))
                first.append(
                    send(m1_ref.at[(z + d) % 4], r1.at[z], as_.at[4 + d], ar.at[4 + d], {"ep_0": (z + d) % 4}))
    kept = [
        pltpu.make_async_copy(m0_ref.at[y], r0.at[y], lsem.at[0]),
        pltpu.make_async_copy(m1_ref.at[z], r1.at[z], lsem.at[1]),
    ]
    for cp in kept:
        cp.start()
    for cp in loads:
        cp.wait()

    def project(block, who):
        at = pl.ds(pl.multiple_of(who * 128, 128), 128)

        def one(j, carry):
            pr_ref[j, at, :] = mm(block, w_s[j])
            return carry

        lax.fori_loop(0, 5, one, 0)

    project(x_ref[...], t)
    passed = []
    for i in range(n // 2):
        for slot, k, peer in ((0, i, right), (1, i + n // 2, left)):
            own[slot, k].wait_recv()
            passed.append(
                send(held.at[slot, rows(k)], held.at[2, rows(k)], fs.at[k], fr.at[k], {"tp": peer}))
    half = pl.ds(pl.multiple_of(c * 128, 128), 128)
    outs = [
        send(wo.at[half], near_ref.at[0], os_.at[0], or_.at[0], {"tp": right}),
        send(wo.at[half], near_ref.at[1], os_.at[1], or_.at[1], {"tp": left}),
    ]
    for cp in kept:
        cp.wait()
    for cp in first:
        cp.wait()
    second = []
    for d in (1, 3, 2):
        second.append(
            send(r0.at[:, (z + d) % 4], s0_ref.at[z], bs.at[d], br.at[d], {"ep_0": (z + d) % 4}))
        second.append(
            send(r1.at[:, (y + d) % 4], s1_ref.at[y], bs.at[4 + d], br.at[4 + d], {"ep_1": (y + d) % 4}))
    kept = [
        pltpu.make_async_copy(r0.at[:, z], s0_ref.at[z], lsem.at[0]),
        pltpu.make_async_copy(r1.at[:, y], s1_ref.at[y], lsem.at[1]),
    ]
    for cp in kept:
        cp.start()
    for i in range(n // 2):
        own[0, i + n // 2].wait_recv()
        own[1, i].wait_recv()
    project(held[0], left)
    project(held[1], right)
    for cp in passed:
        cp.wait()
    project(held[2], (t + 2) % 4)
    for cp in own.values():
        cp.wait_send()
    for cp in kept + second + outs:
        cp.wait()


def expert_kernel(
    t0_ref, t1_ref, g_hbm, u_hbm, d_hbm, near_hbm, res_ref, far_hbm, other_hbm,
    x_s, g_s, u_s, d_s, h_s, g_sem, u_sem, d_sem, fs, fr, cs, cr,
):
    t, c = lax.axis_index("tp"), lax.axis_index("ep_2")
    right, left = (t + 1) % 4, (t + 3) % 4
    loads = []
    for j in range(4):
        for src, dst, sem in ((g_hbm, g_s, g_sem), (u_hbm, u_s, u_sem)):
            pltpu.make_async_copy(src.at[:, j * 256 : (j + 1) * 256], dst.at[j], sem.at[j]).start()
    for j in range(4):
        pltpu.make_async_copy(d_hbm.at[:, j * 512 : (j + 1) * 512], d_s.at[j], d_sem.at[j]).start()
    signal_all([{"tp": right}, {"tp": left}, {"ep_2": 1 - c}])
    passed = [
        send(near_hbm.at[0, 0:64], far_hbm.at[0:64], fs.at[0], fr.at[0], {"tp": right}),
        send(near_hbm.at[1, 64:128], far_hbm.at[64:128], fs.at[1], fr.at[1], {"tp": left}),
    ]
    shared = [send(near_hbm.at[i], other_hbm.at[i], cs.at[i], cr.at[i], {"ep_2": 1 - c}) for i in range(2)]
    order = order_mask(False)
    for i in range(8):
        one = t0_ref[i].reshape(256, 256)
        two = jnp.concatenate([t1_ref[i, y, z] for z in range(4) for y in range(4)], axis=0)
        unpack_block(order, jnp.concatenate([one, two], axis=1), x_s, i)

    def hidden(j, carry):
        pltpu.make_async_copy(g_s.at[j], g_s.at[j], g_sem.at[j]).wait()
        pltpu.make_async_copy(u_s.at[j], u_s.at[j], u_sem.at[j]).wait()
        gate = mm(x_s[...], g_s[j])
        up = mm(x_s[...], u_s[j])
        h_s[j] = (gate / (1.0 + jnp.exp(-gate)) * up).astype(BF)
        return carry

    lax.fori_loop(0, 4, hidden, 0)
    for j in range(4):
        pltpu.make_async_copy(d_s.at[j], d_s.at[j], d_sem.at[j]).wait()
    for j in range(4):
        acc = None
        for f in range(4):
            part = mm(h_s[f], d_s[j, f * 256 : (f + 1) * 256, :])
            acc = part if acc is None else acc + part
        x_s[:, j * 512 : (j + 1) * 512] = acc.astype(BF)
    back = order_mask(True)
    for i in range(8):
        rows_out = jnp.concatenate(
            [x_s[i * 64 : (i + 1) * 64, q * 512 : (q + 1) * 512] for q in range(4)], axis=0)
        units = mm(back, rows_out).astype(BF).reshape(16, 16, 512)
        for k in range(16):
            res_ref[k * 8 + i] = units[k]
    for cp in passed:
        cp.wait()
    shared.append(send(far_hbm, other_hbm.at[2], cs.at[2], cr.at[2], {"ep_2": 1 - c}))
    for cp in shared:
        cp.wait()


def combine_kernel(msg_ref, w_ref, shared_ref, res_ref, x_s):
    order = order_mask(False)
    for i in range(8):
        unpack_block(order, msg_ref[i * 16 : (i + 1) * 16].reshape(256, 512), x_s, i)
    for j in range(4):
        cols = slice(j * 512, (j + 1) * 512)
        both = mm_tn(w_ref[...], x_s[:, cols])
        res_ref[:, cols] = (both[:128] + both[128:] + shared_ref[:, cols]).astype(BF)


def vspec(n):
    return [pl.BlockSpec(memory_space=VMEM)] * n


def per_device(
    mixer_input_rows, mixer_norm_scale, decay_bias_table, erase_bias_table,
    receive_weight, key_weight, value_weight, decay_weight, erase_weight,
    self_token_scale, head_norm_scale, output_weight,
    expert_input_rows, expert_norm_scale, routes, router_weights,
    routed_gate_weight, routed_up_weight, routed_down_weight,
    common_gate_weight, common_up_weight, common_down_weight,
):
    any_spec = pl.BlockSpec(memory_space=pl.ANY)
    sds = jax.ShapeDtypeStruct
    dma = pltpu.SemaphoreType.DMA
    m_shape = sds((4, 4, 8, 16, 256), BF)
    normed_a, normed_b, m0, m1, weights = pl.pallas_call(
        prep_kernel,
        out_shape=(sds((128, 2048), BF), sds((128, 2048), BF), m_shape, m_shape, sds((512, 256), BF)),
        in_specs=vspec(6),
        out_specs=tuple(vspec(5)),
        cost_estimate=pl.CostEstimate(flops=1_000_000_000, bytes_accessed=5_000_000, transcendentals=0),
        name="prep",
    )(mixer_input_rows, mixer_norm_scale.reshape(1, -1), expert_input_rows,
      expert_norm_scale.reshape(1, -1), routes.T, router_weights.T)

    projected, s0, s1, near = pl.pallas_call(
        ring_kernel,
        out_shape=(sds((5, 512, 256), F32), m_shape, m_shape, sds((2, 128, 2048), BF)),
        in_specs=vspec(3) + [any_spec] * 6,
        out_specs=(vspec(1)[0], any_spec, any_spec, any_spec),
        scratch_shapes=[
            VMEM((3, 128, 2048), BF), VMEM((4, 4, 8, 16, 256), BF), VMEM((4, 4, 8, 16, 256), BF),
            VMEM((5, 2048, 256), BF), dma((5,)),
            dma((8,)), dma((8,)), dma((4,)), dma((4,)), dma((8,)), dma((8,)), dma((8,)), dma((8,)),
            dma((2,)), dma((2,)), dma((2,)),
        ],
        compiler_params=pltpu.CompilerParams(collective_id=1, has_side_effects=True),
        cost_estimate=pl.CostEstimate(flops=12_000_000_000, bytes_accessed=8_000_000, transcendentals=0),
        name="ring_project",
    )(normed_a, m0, m1, receive_weight, key_weight, value_weight, decay_weight, erase_weight, output_weight)

    t_shape = sds((8, 4, 4, 16, 256), BF)
    out_l, rt, selft, enter, t0, t1 = pl.pallas_call(
        mixer_kernel,
        out_shape=(sds((512, 256), F32), sds((512, 256), BF), sds((512, 256), F32), sds((64, 256), BF),
                   t_shape, t_shape),
        in_specs=vspec(4) + [any_spec] * 2,
        out_specs=tuple(vspec(4)) + (any_spec, any_spec),
        scratch_shapes=[
            VMEM((512, 256), BF), VMEM((1024, 256), BF), VMEM((1024, 256), F32), VMEM((64, 256), F32),
            VMEM((512, 256), F32), VMEM((128, 256), BF), VMEM((2, 4, 4, 16, 256), BF),
            dma((16,)), dma((16,)), dma((2,)),
            VMEM((128, 256), BF), VMEM((128, 256), BF), VMEM((4, 128, 256), BF),
            VMEM((128, 256), BF), VMEM((4, 128, 256), BF),
            dma, dma, dma((4,)), dma((4,)), dma((4,)), dma((4,)),
        ],
        compiler_params=pltpu.CompilerParams(collective_id=0, has_side_effects=True),
        cost_estimate=pl.CostEstimate(flops=6_000_000_000, bytes_accessed=6_000_000, transcendentals=0),
        name="mixer_state",
    )(projected, decay_bias_table.T, erase_bias_table.reshape(1, 4), self_token_scale, s0, s1)

    result, far, other = pl.pallas_call(
        expert_kernel,
        out_shape=(sds((128, 16, 512), BF), sds((128, 2048), BF), sds((3, 128, 2048), BF)),
        in_specs=vspec(2) + [any_spec] * 4,
        out_specs=(vspec(1)[0], any_spec, any_spec),
        scratch_shapes=[
            VMEM((512, 2048), BF),
            VMEM((4, 2048, 256), BF), VMEM((4, 2048, 256), BF), VMEM((4, 1024, 512), BF),
            VMEM((4, 512, 256), BF),
            dma((4,)), dma((4,)), dma((4,)), dma((2,)), dma((2,)), dma((3,)), dma((3,)),
        ],
        compiler_params=pltpu.CompilerParams(collective_id=2, has_side_effects=True),
        cost_estimate=pl.CostEstimate(flops=8_000_000_000, bytes_accessed=16_000_000, transcendentals=0),
        name="experts",
    )(t0, t1, routed_gate_weight[0], routed_up_weight[0], routed_down_weight[0], near)
    returned = lax.all_to_all(result, EP_TP, split_axis=0, concat_axis=0, tiled=True)

    mixer_output = pl.pallas_call(
        finish_kernel,
        out_shape=sds((128, 2048), BF),
        in_specs=vspec(5) + [any_spec] * 4,
        out_specs=vspec(1)[0],
        scratch_shapes=[
            VMEM((512, 256), BF), VMEM((4, 128, 256), BF), VMEM((4, 256, 2048), BF),
            dma((7,)), dma((4,)), dma((4,)),
        ],
        compiler_params=pltpu.CompilerParams(collective_id=3, has_side_effects=True),
        cost_estimate=pl.CostEstimate(flops=5_000_000_000, bytes_accessed=6_000_000, transcendentals=0),
        name="mixer_finish",
    )(out_l, rt, selft, enter, head_norm_scale.reshape(1, 256), output_weight, near, far, other)

    shared_hidden = (
        jax.nn.silu(jnp.dot(normed_b, common_gate_weight, preferred_element_type=F32))
        * jnp.dot(normed_b, common_up_weight, preferred_element_type=F32)
    ).astype(BF)
    shared_term = jnp.dot(shared_hidden, common_down_weight, preferred_element_type=F32)
    mixed_b = pl.pallas_call(
        combine_kernel,
        out_shape=sds((128, 2048), BF),
        in_specs=vspec(3),
        out_specs=vspec(1)[0],
        scratch_shapes=[VMEM((512, 2048), BF)],
        cost_estimate=pl.CostEstimate(flops=1_000_000_000, bytes_accessed=4_000_000, transcendentals=0),
        name="combine",
    )(returned, weights, shared_term)
    return (mixer_output, mixed_b)


def solution(mesh):
    split = Mesh(mesh.devices.reshape(4, 4, 2, mesh.shape["tp"]), ("ep_0", "ep_1", "ep_2", "tp"))
    in_specs = (
        P(EP_TP, None), P(), P(EP, "tp"), P("tp"),
        P(None, "tp"), P(None, "tp"), P(None, "tp"), P(None, "tp"), P(None, "tp"),
        P("tp", None), P("tp"), P("tp", None),
        P(EP_TP, None), P(), P(EP_TP, None), P(EP_TP, None),
        P(EP_TP, None, None), P(EP_TP, None, None), P(EP_TP, None, None),
        P(), P(), P(),
    )
    out_specs = (P(EP_TP, None), P(EP_TP, None))
    return jax.shard_map(
        per_device, mesh=split, in_specs=in_specs, out_specs=out_specs, check_vma=False
    )
```

time: 158 us -> 139 us (0.88)
  starting transfers between devices: 20.3 us -> 6.54 us
  local copies, waits for them, and re-layouts: 9.68 us -> 3.24 us
  Pallas kernels: 122 us -> 124 us
    pallas_call x3 -> x2, Pallas kernels: 92.8 us -> 54.2 us  [the longest x1 39.2 us: per_device(): pl.pallas_call(ring_kernel, out_shape=(sds((5, 512, 256), F32), m_shape,...]
    pallas_call x1, Pallas kernels: 8.75 us -> 29.5 us  [per_device(): pl.pallas_call(finish_kernel, out_shape=sds((128, 2048), BF), in_specs=vs...]
    pallas_call x1, Pallas kernels: 11.5 us -> 31.6 us  [per_device(): pl.pallas_call(mixer_kernel, out_shape=(sds((512, 256), F32), sds((512, 2...]
    all_to_all x1 -> x0, starting transfers between devices: 11.5 us -> none  [per_device(): lax.all_to_all(outgoing, EP_TP, split_axis=0, concat_axis=0, tiled=True)]
    unnamed x16 -> x5, local copies, waits for them, and re-layouts: 8.3 us -> 3.24 us
    all_to_all x1, starting transfers between devices: 8.79 us -> 6.54 us  [per_device(): lax.all_to_all(result, EP_TP, split_axis=0, concat_axis=0, tiled=True)]
  transfers between devices with their start and end apart: 2 -> 1, of which waited for: 0 -> 0; matrix products, arithmetic and copies ran while one was open for 5% -> 3% of each run, Pallas kernels for 54% -> 21%
where the time goes in v3:
time: 139 us
  Pallas kernels  124 us (89%)
  starting transfers between devices  6.54 us (5%)
  matrix products  4.86 us (3%)
  local copies, waits for them, and re-layouts  3.24 us (2%)
    pallas_call x1, Pallas kernels, per_device(): pl.pallas_call(ring_kernel, out_shape=(sds((5, 512, 256), F32), m_shape,...  39.2 us
    pallas_call x1, Pallas kernels, per_device(): pl.pallas_call(mixer_kernel, out_shape=(sds((512, 256), F32), sds((512, 2...  31.6 us
    pallas_call x1, Pallas kernels, per_device(): pl.pallas_call(finish_kernel, out_shape=sds((128, 2048), BF), in_specs=vs...  29.5 us
    pallas_call x1, Pallas kernels, per_device(): pl.pallas_call(expert_kernel, out_shape=(sds((128, 16, 512), BF), sds((12...  15 us
    all_to_all x1, starting transfers between devices, per_device(): lax.all_to_all(result, EP_TP, split_axis=0, concat_axis=0, tiled=True)  6.54 us
    pallas_call x1, Pallas kernels, per_device(): pl.pallas_call(prep_kernel, out_shape=(sds((128, 2048), BF), sds((128, 20...  4.43 us
    pallas_call x1, Pallas kernels, per_device(): pl.pallas_call(combine_kernel, out_shape=sds((128, 2048), BF), in_specs=v...  4.01 us
    unnamed x5, local copies, waits for them, and re-layouts  3.24 us
  transfers between devices with their start and end apart: 1, of which 0 were waited for; matrix products, arithmetic and copies ran while one was open for 3% of the time, Pallas kernels for 21%

profile of v3, /device:TPU:1, one launch (start us, length us, event | category | flops | bytes accessed | tf_op | source)
XLA Modules:
  0.0 139.0 jit_solution(10018532214157189789)
XLA Ops:
  0.6 0.0 copy-start
  0.6 4.4 %prep.1 = (bf16[128,2048]{1,0:T(8,128)(2,1)}, bf16[128,2048]{1,0:T(8,128)(2,1)}, bf16[4,4,8,16,256]{4,3,2,1,0:T(8,128)(2,1)}, bf16[4,4,8,16,256]{4,3,2,1,0:T(8,128)(2,1)}, bf16[512,256]{1,0:T(8,128)(2,1)}) custom-call(bf16[128,2048]{1,0:T(8,128)(2,1)} %a_ref.1, f32[1,2048]{1,0:T(1,128)} %bitcast.18, bf16[128,2048]{1,0:T(8,128)(2,1)} %b_ref.1, ...), custom_call_target="tpu_custom_call" | custom-call | flops 1000000000 | bytes 5000000 | tf_op jit(solution)/shard_map/prep/pallas_call | solution.py:558
  5.1 39.2 %ring_project.1 = (f32[5,512,256]{2,1,0:T(8,128)}, bf16[4,4,8,16,256]{4,3,2,1,0:T(8,128)(2,1)}, bf16[4,4,8,16,256]{4,3,2,1,0:T(8,128)(2,1)}, bf16[2,128,2048]{2,1,0:T(8,128)(2,1)}) custom-call(bf16[128,2048]{1,0:T(8,128)(2,1)} %get-tuple-element.20.x_ref, bf16[4,4,8,16,256]{4,3,2,1,0:T(8,128)(2,1)} %get-tuple-element.21.m0_ref, ...), custom_call_target="tpu_custom_call" | custom-call | flops 12000000000 | bytes 8000000 | tf_op jit(solution)/shard_map/ring_project/pallas_call | solution.py:568
  44.3 31.6 %mixer_state.1 = (f32[512,256]{1,0:T(8,128)}, bf16[512,256]{1,0:T(8,128)(2,1)}, f32[512,256]{1,0:T(8,128)}, bf16[64,256]{1,0:T(8,128)(2,1)}, bf16[8,4,4,16,256]{...) custom-call(f32[5,512,256]{2,1,0:T(8,128)} %get-tuple-element.23.pr_ref, f32[4,512]{1,0:T(4,128)} %bitcast.20, ...), custom_call_target="tpu_custom_call" | custom-call | flops 6000000000 | bytes 6000000 | tf_op jit(solution)/shard_map/mixer_state/pallas_call | solution.py:585
  75.9 15.0 %experts.1 = (bf16[128,16,512]{2,1,0:T(8,128)(2,1)}, bf16[128,2048]{1,0:T(8,128)(2,1)}, bf16[3,128,2048]{2,1,0:T(8,128)(2,1)}) custom-call(bf16[8,4,4,16,256]{4,3,2,1,0:T(8,128)(2,1)} %get-tuple-element.31.t0_ref, bf16[8,4,4,16,256]{4,3,2,1,0:T(8,128)(2,1)} %get-tuple-element.32.t1_ref, bf16[2048,1024]{1,0:T(8,128)(2,1)} %bitcast.15, ...), custom_call_target="tpu_custom_call" | custom-call | flops 8000000000 | bytes 16000000 | tf_op jit(solution)/shard_map/experts/pallas_call | solution.py:604
  90.9 6.5 %all-to-all-start = ((bf16[128,16,512]{2,1,0:T(8,128)(2,1)}), bf16[128,16,512]{2,1,0:T(8,128)(2,1)S(1)}, u32[]{:S(2)}, u32[]{:S(2)}) async-start(bf16[128,16,512]{2,1,0:T(8,128)(2,1)} %get-tuple-element.35), calls=%async_computation | async-start | bytes 4194304 | tf_op jit(solution)/shard_map/all_to_all | solution.py:619
  97.4 29.5 %mixer_finish.1 = bf16[128,2048]{1,0:T(8,128)(2,1)} custom-call(f32[512,256]{1,0:T(8,128)} %get-tuple-element.26.out_ref, bf16[512,256]{1,0:T(8,128)(2,1)} %get-tuple-element.27.rt_ref, f32[512,256]{1,0:T(8,128)} %get-tuple-element.28.self_ref, bf16[64,256]{1,0:T(8,128)(2,1)} %get-tuple-element.29.enter_ref, f32[1,256]{1,0:T(1,128)} %bitcast.23, ...), custom_call_target="tpu_custom_call" | custom-call | flops 5000000000 | bytes 6000000 | tf_op jit(solution)/shard_map/mixer_finish/pallas_call | solution.py:621
  126.9 1.7 %fusion.9 = f32[128,256]{1,0:T(8,128)S(1)} fusion(bf16[128,2048]{1,0:T(8,128)(2,1)} %get-tuple-element.37, bf16[2048,256]{1,0:T(8,128)(2,1)} %param.41), kind=kOutput, calls=%fused_computation.10 | convolution fusion | flops 134217728 | bytes 1703936 | tf_op jit(solution)/shard_map/dot_general | solution.py:636
  128.6 0.0 copy-done
  128.6 3.2 %fusion.1.shared_ref = f32[128,2048]{1,0:T(8,128)} fusion(bf16[256,2048]{1,0:T(8,128)(2,1)S(1)} %copy-done, bf16[128,2048]{1,0:T(8,128)(2,1)} %get-tuple-element.37, bf16[2048,256]{1,0:T(8,128)(2,1)} %param.42, f32[128,256]{1,0:T(8,128)S(1)} %fusion.9), kind=kOutput, calls=%fused_computation.2 | convolution fusion | flops 268632064 | bytes 3801088 | tf_op jit(solution)/shard_map/dot_general | solution.py:639
  131.8 0.0 all-to-all-done.msg_ref
  131.8 0.0 copy-start.1
  131.8 1.3 copy-done.1
  133.1 4.0 %combine.1 = bf16[128,2048]{1,0:T(8,128)(2,1)} custom-call(bf16[128,16,512]{2,1,0:T(8,128)(2,1)} %copy-done.1, bf16[512,256]{1,0:T(8,128)(2,1)} %get-tuple-element.36.w_ref, f32[128,2048]{1,0:T(8,128)} %fusion.1.shared_ref), custom_call_target="tpu_custom_call" | custom-call | flops 1000000000 | bytes 4000000 | tf_op jit(solution)/shard_map/combine/pallas_call | solution.py:640
  137.2 1.9 %copy.25 = bf16[128,2048]{1,0:T(8,128)(2,1)} copy(bf16[128,2048]{1,0:T(8,128)(2,1)} %mixer_finish.1) | data formatting | bytes 1048576
Async XLA Ops:
  0.6 128.0 %copy-start = (bf16[256,2048]{1,0:T(8,128)(2,1)S(1)}, bf16[256,2048]{1,0:T(8,128)(2,1)}, u32[]{:S(2)}) copy-start(bf16[256,2048]{1,0:T(8,128)(2,1)} %param.43) | copy-start | bytes 3145732
  90.9 40.9 %all-to-all-start = ((bf16[128,16,512]{2,1,0:T(8,128)(2,1)}), bf16[128,16,512]{2,1,0:T(8,128)(2,1)S(1)}, u32[]{:S(2)}, u32[]{:S(2)}) async-start(bf16[128,16,512]{2,1,0:T(8,128)(2,1)} %get-tuple-element.35), calls=%async_computation | async-start | bytes 4194304 | tf_op jit(solution)/shard_map/all_to_all | solution.py:619
  131.8 1.3 copy-start.1

commit v4 on v3

--- a/solution.py
+++ b/solution.py
@@ -269,11 +269,62 @@
     enter_ref[...] = enter.astype(BF)
 
 
+PARTS = ("xyz", "yzx", "zxy", "xyz")
+SIZES = {"x": 8, "y": 4, "z": 4}
+
+
+def part_shape(part, stage):
+    names = part[:stage][::-1] + part[stage:]
+    return tuple(SIZES[a] for a in names) + (16, 128)
+
+
 def finish_kernel(
-    out_ref, rt_ref, self_ref, enter_ref, gain_ref, w_hbm, near_hbm, far_hbm, other_hbm, res_ref,
-    heads, landed, w_s, w_sem, ss, rs,
+    out_ref, rt_ref, self_ref, enter_ref, gain_ref, nb_ref,
+    p0, p1, p2, p3, w_hbm, near_hbm, far_hbm, other_hbm, cg_hbm, cu_hbm, cd_hbm,
+    res_ref, shared_ref, q0, q1, q2, q3,
+    heads, landed, w_s, cg, cu, cd, *rest,
 ):
-    t, c = lax.axis_index("tp"), lax.axis_index("ep_2")
+    mids, (w_sem, c_sem, hs, hr, ss, rs, ls) = rest[:8], rest[8:]
+    z, y, c = lax.axis_index("ep_0"), lax.axis_index("ep_1"), lax.axis_index("ep_2")
+    t = lax.axis_index("tp")
+    signal_all(
+        [{"ep_2": (c + dc) % 2, "tp": (t + dt) % 4} for dc in range(2) for dt in range(4) if dc or dt]
+        + [{"ep_1": (y + d) % 4} for d in range(1, 4)]
+        + [{"ep_0": (z + d) % 4} for d in range(1, 4)]
+    )
+    refs = [
+        (p0, mids[0], mids[1], q0), (p1, mids[2], mids[3], q1),
+        (p2, mids[4], mids[5], q2), (p3, mids[6], mids[7], q3),
+    ]
+
+    def go(part, stage):
+        src, dst = refs[part][stage], refs[part][stage + 1]
+        axis = PARTS[part][stage]
+        cut = lambda who: src.at[(slice(None),) * stage + (who,)]
+        out = []
+        if axis == "x":
+            me = c * 4 + t
+            for dt, dc in ((1, 0), (3, 1), (1, 1), (3, 0), (2, 0), (2, 1), (0, 1)):
+                pc, pt = (c + dc) % 2, (t + dt) % 4
+                at = dc * 4 + dt
+                out.append(send(cut(pc * 4 + pt), dst.at[me], ss.at[part, stage, at], rs.at[part, stage, at],
+                                {"ep_2": pc, "tp": pt}))
+        else:
+            name, me = ("ep_1", y) if axis == "y" else ("ep_0", z)
+            for d in (1, 3, 2):
+                peer = (me + d) % 4
+                out.append(send(cut(peer), dst.at[me], ss.at[part, stage, d], rs.at[part, stage, d], {name: peer}))
+        own = pltpu.make_async_copy(cut(me), dst.at[me], ls.at[part, stage])
+        own.start()
+        return out + [own]
+
+    def finish(copies):
+        for cp in copies:
+            cp.wait()
+
+    a0, b0, c0, d0 = go(0, 0), go(1, 0), go(2, 0), go(3, 0)
+    shared_w = [pltpu.make_async_copy(src, dst, c_sem.at[i])
+                for i, (src, dst) in enumerate(((cg_hbm, cg), (cu_hbm, cu), (cd_hbm, cd)))]
     mine = pl.ds(pl.multiple_of(c * 128, 128), 128)
     theirs = pl.ds(pl.multiple_of((1 - c) * 128, 128), 128)
     loads = [pltpu.make_async_copy(w_hbm, w_s.at[t], w_sem.at[0])]
@@ -281,11 +332,8 @@
         who = (t + (3, 1, 2)[i]) % 4
         loads.append(pltpu.make_async_copy(src, w_s.at[who, mine], w_sem.at[1 + i]))
         loads.append(pltpu.make_async_copy(other_hbm.at[i], w_s.at[who, theirs], w_sem.at[4 + i]))
-    for cp in loads:
+    for cp in shared_w + loads:
         cp.start()
-    barrier = pltpu.get_barrier_semaphore()
-    for d in range(1, 4):
-        pl.semaphore_signal(barrier, inc=1, device_id={"tp": (t + d) % 4}, device_id_type=MESH)
     mask = pair_mask().astype(F32).astype(BF)
     for p in range(2):
         lanes = slice(p * PAIR, (p + 1) * PAIR)
@@ -295,24 +343,45 @@
         var = head_sums(o * o, mask) * (1.0 / 64)
         h = o * lax.rsqrt(var + 0.00064) * gain_ref[:, lanes] + self_ref[:, lanes]
         heads[:, lanes] = h.astype(BF)
-    pl.semaphore_wait(barrier, 3)
     copies = []
     for d in (2, 1, 3):
         peer = (t + d) % 4
         copies.append(
-            send(heads.at[pl.ds(pl.multiple_of(peer * 128, 128), 128)], landed.at[d], ss.at[d], rs.at[d],
+            send(heads.at[pl.ds(pl.multiple_of(peer * 128, 128), 128)], landed.at[d], hs.at[d], hr.at[d],
                  {"tp": peer}))
-    for cp in loads:
-        cp.wait()
+    finish(b0)
+    b1 = go(1, 1)
+    finish(c0)
+    c1 = go(2, 1)
+    finish(a0)
+    a1 = go(0, 1)
+    finish(shared_w)
+    gate = mm(nb_ref[...], cg[...])
+    hid = (gate / (1.0 + jnp.exp(-gate)) * mm(nb_ref[...], cu[...])).astype(BF)
+    for j in range(4):
+        cols = slice(j * 512, (j + 1) * 512)
+        shared_ref[:, cols] = mm(hid, cd[:, cols])
+    finish(d0)
+    d1 = go(3, 1)
+    finish(b1)
+    b2 = go(1, 2)
+    finish(a1)
+    a2 = go(0, 2)
+    finish(c1)
+    c2 = go(2, 2)
+    finish(d1)
+    d2 = go(3, 2)
+    finish(loads)
     own = heads[pl.ds(pl.multiple_of(t * 128, 128), 128), :]
-    for cp in copies:
-        cp.wait()
+    finish(copies)
     for j in range(4):
         cols = slice(j * 512, (j + 1) * 512)
         total = mm(own, w_s[t, :, cols])
         for d in range(1, 4):
             total = total + mm(landed[d], w_s[(t + 4 - d) % 4, :, cols])
         res_ref[:, cols] = total.astype(BF)
+    for copies in (a2, b2, c2, d2):
+        finish(copies)
 
 
 def prep_kernel(a_ref, ga_ref, b_ref, gb_ref, routes_ref, rw_ref, na_ref, nb_ref, m0_ref, m1_ref, w_ref):
@@ -475,7 +544,7 @@
 
 
 def expert_kernel(
-    t0_ref, t1_ref, g_hbm, u_hbm, d_hbm, near_hbm, res_ref, far_hbm, other_hbm,
+    t0_ref, t1_ref, g_hbm, u_hbm, d_hbm, near_hbm, p0_ref, p1_ref, p2_ref, p3_ref, far_hbm, other_hbm,
     x_s, g_s, u_s, d_s, h_s, g_sem, u_sem, d_sem, fs, fr, cs, cr,
 ):
     t, c = lax.axis_index("tp"), lax.axis_index("ep_2")
@@ -521,7 +590,11 @@
             [x_s[i * 64 : (i + 1) * 64, q * 512 : (q + 1) * 512] for q in range(4)], axis=0)
         units = mm(back, rows_out).astype(BF).reshape(16, 16, 512)
         for k in range(16):
-            res_ref[k * 8 + i] = units[k]
+            z, y = k // 4, k % 4
+            p0_ref[i, y, z] = units[k, :, 0:128]
+            p1_ref[y, z, i] = units[k, :, 128:256]
+            p2_ref[z, i, y] = units[k, :, 256:384]
+            p3_ref[i, y, z] = units[k, :, 384:512]
     for cp in passed:
         cp.wait()
     shared.append(send(far_hbm, other_hbm.at[2], cs.at[2], cr.at[2], {"ep_2": 1 - c}))
@@ -529,10 +602,16 @@
         cp.wait()
 
 
-def combine_kernel(msg_ref, w_ref, shared_ref, res_ref, x_s):
+def combine_kernel(q0, q1, q2, q3, w_ref, shared_ref, mixer_ref, pass_ref, res_ref, x_s):
+    pass_ref[...] = mixer_ref[...]
     order = order_mask(False)
     for i in range(8):
-        unpack_block(order, msg_ref[i * 16 : (i + 1) * 16].reshape(256, 512), x_s, i)
+        z, ys = i // 2, (2 * (i % 2), 2 * (i % 2) + 1)
+        cols = [q0[z, ys[0] : ys[0] + 2].reshape(256, 128)]
+        cols.append(jnp.concatenate([q1[x, z, y] for y in ys for x in range(8)], axis=0))
+        cols.append(jnp.concatenate([q2[y, x, z] for y in ys for x in range(8)], axis=0))
+        cols.append(q3[z, ys[0] : ys[0] + 2].reshape(256, 128))
+        unpack_block(order, jnp.concatenate(cols, axis=1), x_s, i)
     for j in range(4):
         cols = slice(j * 512, (j + 1) * 512)
         both = mm_tn(w_ref[...], x_s[:, cols])
@@ -601,11 +680,13 @@
         name="mixer_state",
     )(projected, decay_bias_table.T, erase_bias_table.reshape(1, 4), self_token_scale, s0, s1)
 
-    result, far, other = pl.pallas_call(
+    p_shapes = [sds(part_shape(part, 0), BF) for part in PARTS]
+    q_shapes = [sds(part_shape(part, 3), BF) for part in PARTS]
+    *parts, far, other = pl.pallas_call(
         expert_kernel,
-        out_shape=(sds((128, 16, 512), BF), sds((128, 2048), BF), sds((3, 128, 2048), BF)),
+        out_shape=(*p_shapes, sds((128, 2048), BF), sds((3, 128, 2048), BF)),
         in_specs=vspec(2) + [any_spec] * 4,
-        out_specs=(vspec(1)[0], any_spec, any_spec),
+        out_specs=(*vspec(4), any_spec, any_spec),
         scratch_shapes=[
             VMEM((512, 2048), BF),
             VMEM((4, 2048, 256), BF), VMEM((4, 2048, 256), BF), VMEM((4, 1024, 512), BF),
@@ -616,36 +697,33 @@
         cost_estimate=pl.CostEstimate(flops=8_000_000_000, bytes_accessed=16_000_000, transcendentals=0),
         name="experts",
     )(t0, t1, routed_gate_weight[0], routed_up_weight[0], routed_down_weight[0], near)
-    returned = lax.all_to_all(result, EP_TP, split_axis=0, concat_axis=0, tiled=True)
-
-    mixer_output = pl.pallas_call(
+
+    mixer_rows, shared_term, *back = pl.pallas_call(
         finish_kernel,
-        out_shape=sds((128, 2048), BF),
-        in_specs=vspec(5) + [any_spec] * 4,
-        out_specs=vspec(1)[0],
+        out_shape=(sds((128, 2048), BF), sds((128, 2048), F32), *q_shapes),
+        in_specs=vspec(6) + [any_spec] * 11,
+        out_specs=(*vspec(2), *[any_spec] * 4),
         scratch_shapes=[
             VMEM((512, 256), BF), VMEM((4, 128, 256), BF), VMEM((4, 256, 2048), BF),
-            dma((7,)), dma((4,)), dma((4,)),
+            VMEM((2048, 256), BF), VMEM((2048, 256), BF), VMEM((256, 2048), BF),
+            *[VMEM(part_shape(part, k), BF) for part in PARTS for k in (1, 2)],
+            dma((7,)), dma((3,)), dma((4,)), dma((4,)), dma((4, 3, 8)), dma((4, 3, 8)), dma((4, 3)),
         ],
         compiler_params=pltpu.CompilerParams(collective_id=3, has_side_effects=True),
         cost_estimate=pl.CostEstimate(flops=5_000_000_000, bytes_accessed=6_000_000, transcendentals=0),
         name="mixer_finish",
-    )(out_l, rt, selft, enter, head_norm_scale.reshape(1, 256), output_weight, near, far, other)
-
-    shared_hidden = (
-        jax.nn.silu(jnp.dot(normed_b, common_gate_weight, preferred_element_type=F32))
-        * jnp.dot(normed_b, common_up_weight, preferred_element_type=F32)
-    ).astype(BF)
-    shared_term = jnp.dot(shared_hidden, common_down_weight, preferred_element_type=F32)
-    mixed_b = pl.pallas_call(
+    )(out_l, rt, selft, enter, head_norm_scale.reshape(1, 256), normed_b, *parts,
+      output_weight, near, far, other, common_gate_weight, common_up_weight, common_down_weight)
+
+    mixer_output, mixed_b = pl.pallas_call(
         combine_kernel,
-        out_shape=sds((128, 2048), BF),
-        in_specs=vspec(3),
-        out_specs=vspec(1)[0],
+        out_shape=(sds((128, 2048), BF), sds((128, 2048), BF)),
+        in_specs=vspec(7),
+        out_specs=tuple(vspec(2)),
         scratch_shapes=[VMEM((512, 2048), BF)],
         cost_estimate=pl.CostEstimate(flops=1_000_000_000, bytes_accessed=4_000_000, transcendentals=0),
         name="combine",
-    )(returned, weights, shared_term)
+    )(*back, weights, shared_term, mixer_rows)
     return (mixer_output, mixed_b)
 
 

time: 139 us -> 134 us (0.964)
  Pallas kernels: 124 us -> 133 us
  starting transfers between devices: 6.54 us -> 0 us
  matrix products: 4.86 us -> 0 us
  local copies, waits for them, and re-layouts: 3.24 us -> 0 us
    pallas_call x3, Pallas kernels: 48.5 us -> 58 us  [the longest x1 38.8 us: per_device(): pl.pallas_call(finish_kernel, out_shape=(sds((128, 2048), BF), sds((128,...]
    all_to_all x1 -> x0, starting transfers between devices: 6.54 us -> none  [per_device(): lax.all_to_all(result, EP_TP, split_axis=0, concat_axis=0, tiled=True)]
    dot_general x2 -> x0, matrix products: 4.86 us -> none  [the longest x1 3.16 us: per_device(): jnp.dot(shared_hidden, common_down_weight, preferred_element_type=F32)]
    unnamed x5 -> x0, local copies, waits for them, and re-layouts: 3.24 us -> none
  transfers between devices with their start and end apart: 1 -> 0, of which waited for: 0 -> 0; matrix products, arithmetic and copies ran while one was open for 3% -> 0% of each run, Pallas kernels for 21% -> 0%
where the time goes in v4:
time: 134 us
  Pallas kernels  133 us (99%)
    pallas_call x1, Pallas kernels, per_device(): pl.pallas_call(ring_kernel, out_shape=(sds((5, 512, 256), F32), m_shape,...  39.2 us
    pallas_call x1, Pallas kernels, per_device(): pl.pallas_call(finish_kernel, out_shape=(sds((128, 2048), BF), sds((128,...  38.8 us
    pallas_call x1, Pallas kernels, per_device(): pl.pallas_call(mixer_kernel, out_shape=(sds((512, 256), F32), sds((512, 2...  31.6 us
    pallas_call x1, Pallas kernels, per_device(): pl.pallas_call(expert_kernel, out_shape=(*p_shapes, sds((128, 2048), BF),...  15 us
    pallas_call x1, Pallas kernels, per_device(): pl.pallas_call(prep_kernel, out_shape=(sds((128, 2048), BF), sds((128, 20...  4.34 us
    pallas_call x1, Pallas kernels, per_device(): pl.pallas_call(combine_kernel, out_shape=(sds((128, 2048), BF), sds((128,...  4.2 us

profile of v4, /device:TPU:1, one launch (start us, length us, event | category | flops | bytes accessed | tf_op | source)
XLA Modules:
  0.0 133.7 jit_solution(8569338219428367680)
XLA Ops:
  0.6 4.3 %prep.1 = (bf16[128,2048]{1,0:T(8,128)(2,1)}, bf16[128,2048]{1,0:T(8,128)(2,1)}, bf16[4,4,8,16,256]{4,3,2,1,0:T(8,128)(2,1)}, bf16[4,4,8,16,256]{4,3,2,1,0:T(8,128)(2,1)}, bf16[512,256]{1,0:T(8,128)(2,1)}) custom-call(bf16[128,2048]{1,0:T(8,128)(2,1)} %a_ref.1, f32[1,2048]{1,0:T(1,128)} %bitcast.13, bf16[128,2048]{1,0:T(8,128)(2,1)} %b_ref.1, ...), custom_call_target="tpu_custom_call" | custom-call | flops 1000000000 | bytes 5000000 | tf_op jit(solution)/shard_map/prep/pallas_call | solution.py:637
  5.0 39.2 %ring_project.1 = (f32[5,512,256]{2,1,0:T(8,128)}, bf16[4,4,8,16,256]{4,3,2,1,0:T(8,128)(2,1)}, bf16[4,4,8,16,256]{4,3,2,1,0:T(8,128)(2,1)}, bf16[2,128,2048]{2,1,0:T(8,128)(2,1)}) custom-call(bf16[128,2048]{1,0:T(8,128)(2,1)} %get-tuple-element.29.x_ref, bf16[4,4,8,16,256]{4,3,2,1,0:T(8,128)(2,1)} %get-tuple-element.30.m0_ref, ...), custom_call_target="tpu_custom_call" | custom-call | flops 12000000000 | bytes 8000000 | tf_op jit(solution)/shard_map/ring_project/pallas_call | solution.py:647
  44.1 31.6 %mixer_state.1 = (f32[512,256]{1,0:T(8,128)}, bf16[512,256]{1,0:T(8,128)(2,1)}, f32[512,256]{1,0:T(8,128)}, bf16[64,256]{1,0:T(8,128)(2,1)}, bf16[8,4,4,16,256]{...) custom-call(f32[5,512,256]{2,1,0:T(8,128)} %get-tuple-element.32.pr_ref, f32[4,512]{1,0:T(4,128)} %bitcast.15, ...), custom_call_target="tpu_custom_call" | custom-call | flops 6000000000 | bytes 6000000 | tf_op jit(solution)/shard_map/mixer_state/pallas_call | solution.py:664
  75.7 15.0 %experts.1 = (bf16[8,4,4,16,128]{4,3,2,1,0:T(8,128)(2,1)}, bf16[4,4,8,16,128]{4,3,2,1,0:T(8,128)(2,1)}, bf16[4,8,4,16,128]{4,3,2,1,0:T(8,128)(2,1)}, bf16[8,4,4,...) custom-call(bf16[8,4,4,16,256]{4,3,2,1,0:T(8,128)(2,1)} %get-tuple-element.40.t0_ref, ...), custom_call_target="tpu_custom_call" | custom-call | flops 8000000000 | bytes 16000000 | tf_op jit(solution)/shard_map/experts/pallas_call | solution.py:685
  90.7 38.8 %mixer_finish.1 = (bf16[128,2048]{1,0:T(8,128)(2,1)}, f32[128,2048]{1,0:T(8,128)}, bf16[4,4,8,16,128]{4,3,2,1,0:T(8,128)(2,1)}, bf16[8,4,4,16,128]{4,3,2,1,0:T(8...) custom-call(f32[512,256]{1,0:T(8,128)} %get-tuple-element.35.out_ref, ...), custom_call_target="tpu_custom_call" | custom-call | flops 5000000000 | bytes 6000000 | tf_op jit(solution)/shard_map/mixer_finish/pallas_call | solution.py:701
  129.5 4.2 %combine.1 = (bf16[128,2048]{1,0:T(8,128)(2,1)}, bf16[128,2048]{1,0:T(8,128)(2,1)}) custom-call(bf16[4,4,8,16,128]{4,3,2,1,0:T(8,128)(2,1)} %get-tuple-element.49.q0, bf16[8,4,4,16,128]{4,3,2,1,0:T(8,128)(2,1)} %get-tuple-element.50.q1, bf16[4,8,4,16,128]{4,3,2,1,0:T(8,128)(2,1)} %get-tuple-element.51.q2, bf16[4,4,8,16,128]{4,3,2,1,0:T(8,128)(2,1)} %get-tuple-element.52.q3, ...), custom_call_target="tpu_custom_call" | custom-call | flops 1000000000 | bytes 4000000 | tf_op jit(solution)/shard_map/combine/pallas_call | solution.py:718
